TPU v7x, 128 devices: a whole 4x4x4 slice. The times are simulated.
128 devices in a mesh: ep: 32 (over z, y, core), tp: 4 (over x).
Axes of the slice: x: 4, y: 4, z: 4, core: 2. Of those that a mesh axis runs over, the one named last changes fastest.
Arguments:
- conv_value: bfloat16 [49152, 2048], P(('ep', 'tp')), may hold values from -6 to 6
- conv_gate: bfloat16 [49152, 2048], P(('ep', 'tp')), may hold values from -6 to 6
- conv_taps: float32 [31, 2048], replicated, may hold values from -1 to 1
- conv_gain: float32 [2048], replicated, may hold values from 0.1 to 1.9
- conv_bias: float32 [2048], replicated, may hold values from -3 to 3
- conv_projection: bfloat16 [2048, 4096], P(None, 'tp'), may hold values from -0.125 to 0.125
- expert_input: bfloat16 [16384, 4096], P('ep'), may hold values from -6 to 6
- expert_gain: float32 [4096], replicated, may hold values from 0.1 to 1.9
- route_experts: int32 [16384, 2], P('ep'), may hold values from 0 to 31, all different within a row; in each aligned block of 128 rows (0 to 127, 128 to 255, ...) at most 16 rows name the same one
- group_gate: float32 [16384], P('ep'), may hold values from 0.3 to 1
- expert_gate: float32 [16384, 2], P('ep'), may hold values from 0.1 to 1
- gate_weight: bfloat16 [32, 4096, 1024], P('ep', None, 'tp'), may hold values from -0.09375 to 0.09375
- up_weight: bfloat16 [32, 4096, 1024], P('ep', None, 'tp'), may hold values from -0.09375 to 0.09375
- down_weight: bfloat16 [32, 1024, 4096], P('ep', None, 'tp'), may hold values from -0.1875 to 0.1875
Outputs:
- conv_out: bfloat16 [49152, 4096], P('ep', 'tp')
- expert_out: bfloat16 [16384, 4096], P('ep', 'tp')
Inputs may be any that keep to these rules, and one draw needn't show every extreme that they name: `route_experts`: each row names 2 different experts; in each aligned block of 128 rows no expert is named more than 16 times, and in some blocks one expert is named exactly 16 times.
All inputs are finite; a program needn't handle non-finite values.
Results may differ from a plain program's by a relative error of at most 0.0071.
Values may be sent and summed in bfloat16 or wider, within the bound.
No kernel may reach another device: no remote copies, remote signals or barrier semaphores. Data moves between devices by JAX's collectives and lax.ppermute only.
A program may use at most 128 MiB of HBM per device.

v0:
```python
import jax
import jax.numpy as jnp
from jax import lax
from jax.sharding import Mesh
from jax.sharding import PartitionSpec as P

EXPERTS = 32
TOP = 2
MOE_DEV = 128
CAP = 16
EP_TP = ("ep_0", "ep_1", "ep_2", "tp")
EP = ("ep_0", "ep_1", "ep_2")


epsilon = 1e-06


def passed_along(value, axis, steps):
    count = lax.axis_size(axis)
    leading, last = (max(0, -steps), min(count, count - steps))
    return lax.ppermute(value, axis, [(source, source + steps) for source in range(leading, last)])


def joined_along(blocks, dim):
    shape = list(blocks.shape[1:])
    shape[dim] *= blocks.shape[0]
    return jnp.moveaxis(blocks, 0, dim).reshape(shape)


def work_in_pieces(x, axis, dim, apply, out_dim):
    size, rows = (lax.axis_size(axis), x.shape[dim])
    count = 2 if rows % 2 == 0 else 1
    outs, length = ([], rows // count)
    for k in range(count):
        section = lax.slice_in_dim(x, k * length, (k + 1) * length, axis=dim)
        starts = jnp.arange(size) * rows + k * length
        outs.append(jax.vmap(apply)(lax.all_gather(section, axis), starts))
    return joined_along(jnp.concatenate(outs, axis=out_dim + 1), out_dim)


def split_up(x, dim, length):
    before, after = (x.shape[:dim], x.shape[dim + 1 :])
    return jnp.moveaxis(x.reshape(*before, length, -1, *after), dim, 0)


def exchange_in_order(blocks, axes, order):
    shape = [lax.axis_size(a) for a in axes]
    blocks = blocks.reshape(*shape, *blocks.shape[1:])
    for k in order:
        blocks = lax.all_to_all(blocks, axes[k], split_axis=k, concat_axis=k, tiled=True)
    return blocks.reshape(-1, *blocks.shape[len(axes) :])


def core_and_chips(x, groups, order, split_dim, concat_dim):
    length = lax.axis_size(groups[0]) * lax.axis_size(groups[1])
    blocks = split_up(x, split_dim, length)
    return joined_along(exchange_in_order(blocks, groups, order), concat_dim)


def root_mean_norm(values, gain):
    widened = values.astype(jnp.float32)
    inverse_rms = lax.rsqrt(jnp.mean(widened * widened, axis=-1, keepdims=True) + epsilon)
    return (widened * inverse_rms * gain).astype(jnp.bfloat16)


def slot_positions(route_block):
    picked_experts = route_block.reshape(route_block.shape[0] // MOE_DEV, MOE_DEV * TOP)
    onehot = (
        picked_experts[:, :, None] == jnp.arange(EXPERTS, dtype=jnp.int32)[None, None, :]
    ).astype(jnp.int32)
    before = jnp.cumsum(onehot, axis=1) - onehot
    return (picked_experts, jnp.sum(before * onehot, axis=2))


def one_table(slot_index, token_index):
    return jnp.full((EXPERTS * CAP,), -1, jnp.int32).at[slot_index].set(token_index)


def take_rows(normed, source):
    return jnp.take(normed, jnp.maximum(source, 0), axis=0)


def fill_slots(normed, picked_experts, positions):
    slot_index = picked_experts * CAP + positions
    token_index = jnp.broadcast_to(
        jnp.arange(MOE_DEV * TOP, dtype=jnp.int32) // TOP, slot_index.shape
    )
    source = jax.vmap(one_table)(slot_index, token_index)
    taken_rows = jax.vmap(take_rows)(normed, source)
    taken_rows = jnp.where((source >= 0)[:, :, None], taken_rows, jnp.zeros_like(taken_rows))
    return taken_rows.reshape(normed.shape[0], EXPERTS, CAP, normed.shape[2])


def on_device(
    conv_value,
    conv_gate,
    conv_taps,
    conv_gain,
    conv_bias,
    conv_projection,
    expert_input,
    expert_gain,
    route_experts,
    group_gate,
    expert_gate,
    gate_weight,
    up_weight,
    down_weight,
):
    gated_rows = (
        conv_value.astype(jnp.float32) * jax.nn.sigmoid(conv_gate.astype(jnp.float32))
    ).astype(jnp.bfloat16)
    reach_back = conv_taps.shape[0] - 1
    length = gated_rows.shape[0]
    earlier = passed_along(gated_rows[length - reach_back :], EP_TP, 1)
    extended = jnp.concatenate([earlier, gated_rows], axis=0)
    mixed_conv = jnp.zeros(gated_rows.shape, jnp.float32)
    for lag_step in range(reach_back + 1):
        window = lax.slice_in_dim(
            extended, reach_back - lag_step, reach_back - lag_step + length, axis=0
        )
        mixed_conv = mixed_conv + conv_taps[lag_step] * window.astype(jnp.float32)
    center = mixed_conv - jnp.mean(mixed_conv, axis=-1, keepdims=True)
    spread = jnp.mean(center * center, axis=-1, keepdims=True)
    activated = jax.nn.silu(center * lax.rsqrt(spread + epsilon) * conv_gain + conv_bias).astype(
        jnp.bfloat16
    )

    def project_rows(piece_rows, start_row):
        return jnp.dot(piece_rows, conv_projection, preferred_element_type=jnp.float32)

    conv_out = work_in_pieces(activated, "tp", 0, project_rows, 0).astype(jnp.bfloat16)
    quarters = lax.axis_size("tp")
    own_quarter = lax.axis_index("tp")
    picked_experts, positions = slot_positions(route_experts)
    own_rows = lax.dynamic_slice_in_dim(expert_input, own_quarter * MOE_DEV, MOE_DEV, 0)
    normed = root_mean_norm(own_rows, expert_gain)[None]
    own_experts = lax.dynamic_slice_in_dim(picked_experts, own_quarter, 1, 0)
    own_positions = lax.dynamic_slice_in_dim(positions, own_quarter, 1, 0)
    outgoing = fill_slots(normed, own_experts, own_positions)
    arrived = lax.all_to_all(outgoing, EP, split_axis=1, concat_axis=2, tiled=True)
    hidden_arrived = lax.all_gather(arrived, "tp", axis=0, tiled=True)
    gate_part = jnp.einsum(
        "qecd,edh->qech", hidden_arrived, gate_weight, preferred_element_type=jnp.float32
    )
    up_part = jnp.einsum(
        "qecd,edh->qech", hidden_arrived, up_weight, preferred_element_type=jnp.float32
    )
    hidden = (jax.nn.silu(gate_part) * up_part).astype(jnp.bfloat16)
    summed = jnp.einsum(
        "qech,ehd->qecd",
        lax.all_gather(hidden, "tp", axis=3, tiled=True),
        down_weight,
        preferred_element_type=jnp.float32,
    )
    returned = core_and_chips(summed.astype(jnp.bfloat16), (("ep_0", "ep_1"), "ep_2"), (1, 0), 2, 1)
    result_table = returned.reshape(quarters * EXPERTS * CAP, returned.shape[3])
    plane_index = jnp.arange(quarters, dtype=jnp.int32)[:, None]
    slot_index = (plane_index * EXPERTS + picked_experts) * CAP + positions
    picked = jnp.take(result_table, slot_index.reshape(-1), axis=0).reshape(
        -1, TOP, returned.shape[3]
    )
    route_share = group_gate[:, None] * expert_gate / jnp.sum(expert_gate, axis=1, keepdims=True)
    expert_out = jnp.sum(picked.astype(jnp.float32) * route_share[:, :, None], axis=1).astype(
        jnp.bfloat16
    )
    return (conv_out, expert_out)


def solution(mesh):
    finer = Mesh(mesh.devices.reshape(4, 4, 2, mesh.shape["tp"]), ("ep_0", "ep_1", "ep_2", "tp"))
    in_specs = (
        P(EP_TP, None),
        P(EP_TP, None),
        P(),
        P(),
        P(),
        P(None, "tp"),
        P(EP, None),
        P(),
        P(EP, None),
        P(EP),
        P(EP, None),
        P(EP, None, "tp"),
        P(EP, None, "tp"),
        P(EP, None, "tp"),
    )
    out_specs = (P(EP, "tp"), P(EP, "tp"))
    return jax.shard_map(
        on_device, mesh=finer, in_specs=in_specs, out_specs=out_specs, check_vma=False
    )
```

profile of v0, /device:TPU:1, one launch (start us, length us, event | category | flops | bytes accessed | tf_op | source)
XLA Modules:
  0.0 446.0 jit_solution(4297248506721945135)
XLA Ops:
  7.2 0.0 copy-start
  7.2 0.0 all-gather.7.cloned.1.call-start
  7.2 1.0 copy.56
  8.2 0.2 eq.29
  8.4 0.2 eq.25
  8.6 2.3 reduce-window.6
  10.9 0.1 slice.331
  11.0 0.1 copy.58
  11.1 0.1 fusion.65
  11.3 1.4 scatter_custom_fusion
  12.8 1.5 fusion.13
  14.3 0.1 broadcast_in_dim.62
  14.4 0.1 broadcast_in_dim.64
  14.5 1.6 fusion.62
  16.1 17.4 %gather_fusion.1 = bf16[512,4096]{1,0:T(8,128)(2,1)} fusion(bf16[1,128,4096]{2,1,0:T(8,128)(2,1)S(1)} %fusion.62, s32[512]{0:T(512)S(1)} %bitcast.161), kind=kCustom, calls=%fused_computation.1 | custom fusion | bytes 8392704 | tf_op jit(solution)/shard_map/vmap(jit(_take))/gather | solution.py:80
  33.5 2.6 select_select_fusion
  36.1 60.3 %all_to_all.22 = bf16[1,32,16,4096]{3,2,0,1:T(8,128)(2,1)} all-to-all(bf16[1,32,16,4096]{3,2,0,1:T(8,128)(2,1)S(1)} %select_select_fusion), channel_id=1, replica_groups=mesh['ep_0'=4,'ep_1'=4,'ep_2'=2,'tp'=4] {'ep_0','ep_1','ep_2'}, dimensions={1} | all-to-all | bytes 8388608 | tf_op jit(solution)/shard_map/all_to_all | solution.py:141
  96.3 0.0 all-gather.7.cloned.1.call-update
  96.3 0.2 all-gather.9.cloned.1.call-start
  96.6 151.2 %all-gather.7.cloned.1.call-done = bf16[4,1,512,4096]{3,2,1,0:T(8,128)(2,1)} async-done(((bf16[1,1,512,4096]{3,2,1,0:T(8,128)(2,1)}), bf16[4,1,512,4096]{3,2,1,0:T(8,128)(2,1)}) %all-gather.7.cloned.1.call-update) | async-done | bytes 16777232 | tf_op jit(solution)/shard_map/all_gather | solution.py:142
  247.8 8.9 %fusion = f32[4,512,256]{2,1,0:T(8,128)S(1)} fusion(bf16[4,1,512,4096]{3,2,1,0:T(8,128)(2,1)} %all-gather.7.cloned.1.call-done, bf16[1,4096,256]{2,1,0:T(8,128)(2,1)} %param.26), kind=kOutput, calls=%fused_computation.32 | convolution fusion | flops 4294967296 | bytes 20971520 | tf_op jit(solution)/shard_map/qecd,edh->qech/dot_general | solution.py:146
  256.7 2.3 copy-done.8
  258.9 0.6 copy-done.9
  259.5 6.0 %fusion.16 = bf16[4,1,512,256]{3,2,0,1:T(8,128)(2,1)} fusion(f32[4,512,256]{2,1,0:T(8,128)S(1)} %fusion, bf16[1,4096,256]{2,1,0:T(8,128)(2,1)S(1)} %copy-done.9, bf16[4,1,512,4096]{3,2,1,0:T(8,128)(2,1)S(1)} %copy-done.8), kind=kOutput, calls=%fused_computation.57 | convolution fusion | flops 4298113024 | bytes 22020096 | tf_op jit(solution)/shard_map/qecd,edh->qech/dot_general | solution.py:143
  265.5 0.0 all-gather.9.cloned.1.call-update
  265.6 0.0 all-gather.11.cloned.1.call-start
  265.6 2.8 multiply_convert_fusion.1
  268.4 3.1 collective-permute-start
  271.5 0.0 copy-done.2
  271.6 0.1 fusion.77
  271.7 0.1 fusion.78
  271.8 4.5 %collective-permute-done = bf16[30,2048]{1,0:T(8,128)(2,1)S(1)} collective-permute-done((bf16[30,2048]{1,0:T(8,128)(2,1)S(1)}, bf16[30,2048]{1,0:T(8,128)(2,1)S(1)}, u32[]{:S(2)}, u32[]{:S(2)}) %collective-permute-start) | collective-permute-done | bytes 122912 | tf_op jit(solution)/shard_map/ppermute | solution.py:21
  276.3 14.3 %fusion.75 = (f32[384]{0:T(512)S(1)}, f32[384,2048]{1,0:T(8,128)S(1)}) fusion(bf16[384,2048]{1,0:T(8,128)(2,1)S(1)} %multiply_convert_fusion.1, bf16[30,2048]{1,0:T(8,128)(2,1)S(1)} %collective-permute-done, f32[2048]{0:T(1024)S(1)} %bitcast.198, f32[2048]{0:T(1024)S(1)} %bitcast.199, f32[2048]{0:T(1024)S(1)} %bitcast.170, f32[2048]{0:T(1024)S(1)} %bitcast.171, ...), kind=kLoop, calls=%fused_computation.145 | loop fusion | flops 143916672 | bytes 5096960 | tf_op jit(solution)/shard_map/reduce_sum | solution.py:123
  290.6 0.5 multiply_reduce_fusion.1
  291.1 1.3 multiply_convert_fusion
  292.4 1.3 fusion.76
  293.6 0.0 all-gather.11.cloned.1.call-update
  293.6 0.3 all-gather.13.cloned.1.call-start
  293.9 0.3 all-gather.13.cloned.1.call-update
  294.2 22.6 %all-gather.9.cloned.1.call-done = bf16[4,1,512,1024]{3,2,0,1:T(8,128)(2,1)} async-done(((bf16[4,1,512,256]{3,2,0,1:T(8,128)(2,1)}), bf16[4,1,512,1024]{3,2,0,1:T(8,128)(2,1)}) %all-gather.9.cloned.1.call-update) | async-done | bytes 4194320 | tf_op jit(solution)/shard_map/all_gather | solution.py:152
  316.8 6.9 %fusion.10 = bf16[4,512,1024]{2,1,0:T(8,128)(2,1)S(1)} fusion(bf16[4,1,512,1024]{3,2,0,1:T(8,128)(2,1)} %all-gather.9.cloned.1.call-done, bf16[1,1024,1024]{2,1,0:T(8,128)(2,1)S(1)} %copy-done), kind=kOutput, calls=%fused_computation.50 | convolution fusion | flops 4297064448 | bytes 10485760 | tf_op jit(solution)/shard_map/qech,ehd->qecd/dot_general | solution.py:150
  323.8 0.8 copy.64
  324.6 0.8 copy.65
  325.4 8.8 %all_to_all.23 = bf16[16,2,4,1,16,1024]{5,4,0,2,3,1:T(8,128)(2,1)S(1)} all-to-all(bf16[16,2,4,1,16,1024]{5,4,0,2,3,1:T(8,128)(2,1)S(1)} %copy.65), channel_id=1, replica_groups=mesh['ep_0'=4,'ep_1'=4,'ep_2'=2,'tp'=4] {'ep_2'}, dimensions={1} | all-to-all | bytes 8388608 | tf_op jit(solution)/shard_map/all_to_all | solution.py:50
  334.2 2.4 copy.66
  336.6 6.9 %all-to-all-start.2 = ((bf16[16,2,4,1,16,1024]{5,4,1,2,3,0:T(8,128)(2,1)}), bf16[16,2,4,1,16,1024]{5,4,1,2,3,0:T(8,128)(2,1)}, u32[]{:S(2)}, u32[]{:S(2)}) async-start(bf16[16,2,4,1,16,1024]{5,4,1,2,3,0:T(8,128)(2,1)} %copy.66), calls=%async_computation.2 | async-start | bytes 8388608 | tf_op jit(solution)/shard_map/all_to_all | solution.py:50
  343.5 0.2 reshape.234
  343.7 0.2 reduce_sum.61
  343.9 0.1 broadcast_bitcast_fusion
  344.0 0.1 copy.61
  344.1 0.1 broadcast_bitcast_fusion.1
  344.2 0.2 copy.62
  344.5 0.1 copy.70
  344.6 16.0 %all-gather.11.cloned.1.call-done = bf16[768,2048]{1,0:T(8,128)(2,1)} async-done(((bf16[192,2048]{1,0:T(8,128)(2,1)}), bf16[768,2048]{1,0:T(8,128)(2,1)}) %all-gather.11.cloned.1.call-update) | async-done | bytes 3145744 | tf_op jit(solution)/shard_map/all_gather | solution.py:37
  360.6 6.6 %fusion.23 = bf16[4,192,1024]{2,1,0:T(8,128)(2,1)S(1)} fusion(bf16[4,192,2048]{2,1,0:T(8,128)(2,1)} %bitcast.205, bf16[2048,1024]{1,0:T(8,128)(2,1)} %param.19), kind=kOutput, calls=%fused_computation.66 | convolution fusion | flops 3222011904 | bytes 8912896 | tf_op jit(solution)/shard_map/vmap()/dot_general | solution.py:130
  367.2 34.6 %all-gather.13.cloned.1.call-done = bf16[768,2048]{1,0:T(8,128)(2,1)} async-done(((bf16[192,2048]{1,0:T(8,128)(2,1)}), bf16[768,2048]{1,0:T(8,128)(2,1)}) %all-gather.13.cloned.1.call-update) | async-done | bytes 3145744 | tf_op jit(solution)/shard_map/all_gather | solution.py:37
  401.8 6.6 %fusion.26 = bf16[4,192,1024]{2,1,0:T(8,128)(2,1)S(1)} fusion(bf16[4,192,2048]{2,1,0:T(8,128)(2,1)} %bitcast.206, bf16[2048,1024]{1,0:T(8,128)(2,1)} %param.19), kind=kOutput, calls=%fused_computation.67 | convolution fusion | flops 3222011904 | bytes 8912896 | tf_op jit(solution)/shard_map/vmap()/dot_general | solution.py:130
  408.4 2.0 pad_maximum_fusion
  410.4 0.0 all-to-all-done.2
  410.4 2.6 copy.67
  413.0 2.4 copy.68
  415.4 8.9 %gather_fusion = bf16[1024,1024]{1,0:T(8,128)(2,1)} fusion(bf16[2048,1024]{1,0:T(8,128)(2,1)} %bitcast.160, s32[1024]{0:T(1024)S(1)} %broadcast_clamp_fusion), kind=kCustom, calls=%fused_computation | custom fusion | bytes 4198400 | tf_op jit(solution)/shard_map/jit(_take)/gather | solution.py:160
  424.3 4.1 gather.15
  428.4 11.0 %multiply_reduce_fusion = bf16[512,1024]{1,0:T(8,128)(2,1)} fusion(bf16[512,2,1024]{2,1,0:T(2,128)(2,1)} %gather.15, pred[512,2]{1,0:T(8,128)(4,1)S(1)} %copy.62, f32[512,2]{1,0:T(8,128)S(1)} %copy.70), kind=kLoop, calls=%fused_computation.42 | loop fusion | flops 3670016 | bytes 3150848 | tf_op jit(solution)/shard_map/reduce_sum | solution.py:164
  (40 shorter events, 0.3 us)
Async XLA Ops:
  7.2 309.7 %copy-start = (bf16[1,1024,1024]{2,1,0:T(8,128)(2,1)S(1)}, bf16[1,1024,1024]{2,1,0:T(8,128)(2,1)}, u32[]{:S(2)}) copy-start(bf16[1,1024,1024]{2,1,0:T(8,128)(2,1)} %param.27) | copy-start | bytes 6291460
  7.2 240.6 %all-gather.7.cloned.1.call-start = ((), (), s32[]{:S(2)}) async-start(), calls=%async_computation.3 | async-start | bytes 20971520 | tf_op jit(solution)/shard_map/all_gather | solution.py:142
  96.3 220.5 %all-gather.9.cloned.1.call-start = ((), (), s32[]{:S(2)}) async-start(), calls=%async_computation.4 | async-start | bytes 5242880 | tf_op jit(solution)/shard_map/all_gather | solution.py:152
  247.8 11.1 %copy-start.8 = (bf16[4,1,512,4096]{3,2,1,0:T(8,128)(2,1)S(1)}, bf16[4,1,512,4096]{3,2,1,0:T(8,128)(2,1)}, u32[]{:S(2)}) copy-start(bf16[4,1,512,4096]{3,2,1,0:T(8,128)(2,1)} %all-gather.7.cloned.1.call-done) | copy-start | bytes 50331652
  247.8 11.7 %copy-start.9 = (bf16[1,4096,256]{2,1,0:T(8,128)(2,1)S(1)}, bf16[1,4096,256]{2,1,0:T(8,128)(2,1)}, u32[]{:S(2)}) copy-start(bf16[1,4096,256]{2,1,0:T(8,128)(2,1)} %param.25) | copy-start | bytes 6291460
  265.5 6.0 %copy-start.2 = (f32[31,2048]{1,0:T(8,128)S(1)}, f32[31,2048]{1,0:T(8,128)}, u32[]{:S(2)}) copy-start(f32[31,2048]{1,0:T(8,128)} %param.16) | copy-start | bytes 761860
  265.6 95.1 %all-gather.11.cloned.1.call-start = ((), (), s32[]{:S(2)}) async-start(), calls=%async_computation.5 | async-start | bytes 3932160 | tf_op jit(solution)/shard_map/all_gather | solution.py:37
  268.4 7.8 %collective-permute-start = (bf16[30,2048]{1,0:T(8,128)(2,1)S(1)}, bf16[30,2048]{1,0:T(8,128)(2,1)S(1)}, u32[]{:S(2)}, u32[]{:S(2)}) collective-permute-start(bf16[30,2048]{1,0:T(8,128)(2,1)S(1)} %slice.270), channel_id=1, source_target_pairs={{0,1},{1,2},{2,3},{3,4},{4,5},{5,6},{6,7},{7,8},{8,9},{9,10},{10,1... | collective-permute-start | bytes 368648 | tf_op jit(solution)/shard_map/ppermute | solution.py:21
  276.3 14.8 %copy-start.5 = (f32[2048]{0:T(1024)S(1)}, f32[2048]{0:T(1024)}, u32[]{:S(2)}) copy-start(f32[2048]{0:T(1024)} %param.18) | copy-start | bytes 24580
  276.3 14.8 %copy-start.6 = (f32[2048]{0:T(1024)S(1)}, f32[2048]{0:T(1024)}, u32[]{:S(2)}) copy-start(f32[2048]{0:T(1024)} %param.17) | copy-start | bytes 24580
  293.6 108.2 %all-gather.13.cloned.1.call-start = ((), (), s32[]{:S(2)}) async-start(), calls=%async_computation.6 | async-start | bytes 3932160 | tf_op jit(solution)/shard_map/all_gather | solution.py:37
  336.6 7.6 %copy-start.3 = (s32[512,2]{0,1:T(2,128)S(1)}, s32[512,2]{0,1:T(2,128)}, u32[]{:S(2)}) copy-start(s32[512,2]{0,1:T(2,128)} %param.22) | copy-start | bytes 12292
  336.6 7.8 %copy-start.4 = (f32[512,2]{0,1:T(2,128)S(1)}, f32[512,2]{0,1:T(2,128)}, u32[]{:S(2)}) copy-start(f32[512,2]{0,1:T(2,128)} %param.24) | copy-start | bytes 12292
  336.6 7.8 %copy-start.7 = (f32[512]{0:T(512)S(1)}, f32[512]{0:T(512)}, u32[]{:S(2)}) copy-start(f32[512]{0:T(512)} %param.23) | copy-start | bytes 6148
  336.6 73.8 %all-to-all-start.2 = ((bf16[16,2,4,1,16,1024]{5,4,1,2,3,0:T(8,128)(2,1)}), bf16[16,2,4,1,16,1024]{5,4,1,2,3,0:T(8,128)(2,1)}, u32[]{:S(2)}, u32[]{:S(2)}) async-start(bf16[16,2,4,1,16,1024]{5,4,1,2,3,0:T(8,128)(2,1)} %copy.66), calls=%async_computation.2 | async-start | bytes 8388608 | tf_op jit(solution)/shard_map/all_to_all | solution.py:50
  415.4 24.1 %copy-start.1 = (bf16[1,1024,1024]{2,1,0:T(8,128)(2,1)S(1)}, bf16[1,1024,1024]{2,1,0:T(8,128)(2,1)}, u32[]{:S(2)}) copy-start(bf16[1,1024,1024]{2,1,0:T(8,128)(2,1)} %param.27) | copy-start | bytes 6291460
Sparse Core Ops, SparseCore 0:
  96.5 151.2 all-gather.6
  265.7 51.1 all-gather.8
  319.1 41.5 all-gather.10
  362.2 39.6 all-gather.12
where the time goes:
time: 447 us; the launch traced here: 446 us
  waiting for transfers between devices  229 us (51%)
  blocking collectives  69 us (15%)
  local copies, waits for them, and re-layouts  47.9 us (11%)
  other arithmetic  40.1 us (9%)
  matrix products  34.9 us (8%)
  between operations  14.1 us (3%)
  starting transfers between devices  10.5 us (2%)
    all_gather x1, waiting for transfers between devices, on_device(): hidden_arrived = lax.all_gather(arrived, 'tp', axis=0, tiled=True)  151 us
    all_to_all x1, blocking collectives, on_device(): lax.all_to_all(outgoing, EP, split_axis=1, concat_axis=2, tiled=True)  60.3 us
    all_gather x2, waiting for transfers between devices, work_in_pieces(): outs.append(jax.vmap(apply)(lax.all_gather(section, axis), starts))  50.6 us
    all_gather x1, waiting for transfers between devices, on_device(): lax.all_gather(hidden, 'tp', axis=3, tiled=True)  22.6 us
    gather x2, local copies, waits for them, and re-layouts, take_rows(): return jnp.take(normed, jnp.maximum(source, 0), axis=0)  17.4 us
    reduce_sum x1, other arithmetic, on_device(): center = mixed_conv - jnp.mean(mixed_conv, axis=-1, keepdims=True)  14.3 us
    dot_general x2, matrix products, project_rows(): jnp.dot(piece_rows, conv_projection, preferred_element_type=jnp.float32)  13.1 us
    gather x2, local copies, waits for them, and re-layouts, on_device(): jnp.take(result_table, slot_index.reshape(-1), axis=0)  13 us
  transfers between devices with their start and end apart: 6, of which 5 were waited for; matrix products, arithmetic and copies ran while one was open for 11% of the time, Pallas kernels for 0%

commit v1 on v0

v1 whole, which is shorter than its diff:
```python
import functools
import jax
import jax.numpy as jnp
from jax import lax
from jax.experimental import pallas as pl
from jax.experimental.pallas import tpu as pltpu
from jax.sharding import Mesh
from jax.sharding import PartitionSpec as P

EXPERTS = 32
TOP = 2
MOE_DEV = 128
CAP = 16
PLANES = 16
CHUNKS = 2
EP_TP = ("ep_0", "ep_1", "ep_2", "tp")
EP = ("ep_0", "ep_1", "ep_2")
CHIPS = ("ep_0", "ep_1")
CORE_TP = ("ep_2", "tp")

epsilon = 1e-06
f32 = jnp.float32
bf16 = jnp.bfloat16


def ring_pairs(move):
    pairs = []
    for core in range(2):
        for x in range(4):
            to_core, to_x = move(core, x)
            pairs.append((core * 4 + x, to_core * 4 + to_x))
    return pairs


def weight_partner(core, x):
    return core, (((x - core) % 4 ^ 1) + core) % 4


def hidden_partner(core, x):
    return core, ((3 - (x - core) % 4) + core) % 4


def other_core(core, x):
    return 1 - core, x


def diagonal(core, x):
    return 1 - core, weight_partner(core, x)[1]


def swapped(value, move):
    return lax.ppermute(value, CORE_TP, ring_pairs(move))


def block_slots(info, core):
    picks = info[:, 0:TOP].astype(jnp.int32)
    first, second = picks[:, 0:1], picks[:, 1:2]
    rows = info.shape[0]
    lanes = lax.broadcasted_iota(jnp.int32, (rows, EXPERTS), 1)
    in_first, in_second = first == lanes, second == lanes
    named = jnp.where(in_first | in_second, 1.0, 0.0).astype(bf16)
    earlier = (
        lax.broadcasted_iota(jnp.int32, (rows, rows), 1)
        < lax.broadcasted_iota(jnp.int32, (rows, rows), 0)
    )
    before = jnp.dot(
        jnp.where(earlier, 1.0, 0.0).astype(bf16), named, preferred_element_type=f32
    )
    slots = []
    for pick, mask in ((first, in_first), (second, in_second)):
        position = jnp.sum(jnp.where(mask, before, 0.0), axis=1, keepdims=True)
        slot = (pick >> 1) * CAP + position.astype(jnp.int32)
        slots.append(jnp.where((pick & 1) == core, slot, -1))
    return slots


def dispatch_kernel(where, own_ref, sib_ref, own_info, sib_info, gain_ref, out_ref):
    core = where[1]
    gain = gain_ref[...]
    width = 512

    def run(x_ref, info_ref):
        widened = x_ref[...].astype(f32)
        depth = widened.shape[1]
        inverse = lax.rsqrt(jnp.mean(widened * widened, axis=-1, keepdims=True) + epsilon)
        slot_a, slot_b = block_slots(info_ref[...], core)
        lanes = lax.broadcasted_iota(jnp.int32, (MOE_DEV, PLANES * CAP), 1)
        table = jnp.where((lanes == slot_a) | (lanes == slot_b), 1.0, 0.0)
        spread = table.T.astype(bf16)
        for k in range(depth // width):
            cols = slice(k * width, (k + 1) * width)
            normed = (x_ref[:, cols].astype(f32) * inverse * gain[:, cols]).astype(bf16)
            rows = jnp.dot(spread, normed, preferred_element_type=f32).astype(bf16)
            out_ref[:, :, cols] = rows.reshape(PLANES, CAP, width)

    @pl.when(pl.program_id(0) == 0)
    def _():
        run(own_ref, own_info)

    @pl.when(pl.program_id(0) == 1)
    def _():
        run(sib_ref, sib_info)


def dispatch(where, expert_input, sib_rows, info, sib_info, gain, chunk):
    depth = expert_input.shape[1]
    per_half = 2
    return pl.pallas_call(
        dispatch_kernel,
        grid_spec=pltpu.PrefetchScalarGridSpec(
            num_scalar_prefetch=1,
            grid=(2,),
            in_specs=[
                pl.BlockSpec((MOE_DEV, depth), lambda i, w: (w[0] * per_half + chunk, 0)),
                pl.BlockSpec((MOE_DEV, depth), lambda i, w: (chunk, 0)),
                pl.BlockSpec((MOE_DEV, 4), lambda i, w: (w[0] * per_half + chunk, 0)),
                pl.BlockSpec((MOE_DEV, 4), lambda i, w: (w[0] * per_half + chunk, 0)),
                pl.BlockSpec((1, depth), lambda i, w: (0, 0)),
            ],
            out_specs=pl.BlockSpec((PLANES, CAP, depth), lambda i, w: (0, i, 0)),
        ),
        out_shape=jax.ShapeDtypeStruct((PLANES, 2 * CAP, depth), bf16),
        cost_estimate=pl.CostEstimate(
            flops=2 * 2 * MOE_DEV * PLANES * CAP * depth * 8,
            bytes_accessed=8 << 20,
            transcendentals=0,
        ),
        name="dispatch",
    )(where, expert_input, sib_rows, info, sib_info, gain)


def combine_kernel(where, own_info, sib_info, result_ref, keep, to_partner, to_sib, to_diag):
    core = where[1]
    half = keep.shape[1]
    for source, info_ref in enumerate((own_info, sib_info)):
        info = info_ref[...]
        slot_a, slot_b = block_slots(info, core)
        lanes = lax.broadcasted_iota(jnp.int32, (MOE_DEV, PLANES * CAP), 1)
        weights = jnp.where(lanes == slot_a, info[:, 2:3], 0.0) + jnp.where(
            lanes == slot_b, info[:, 3:4], 0.0
        )
        coarse = weights.astype(bf16)
        fine = (weights - coarse.astype(f32)).astype(bf16)
        for part in range(2):
            table = result_ref[
                :, source * CAP : (source + 1) * CAP, part * half : (part + 1) * half
            ].reshape(PLANES * CAP, half)
            total = jnp.dot(coarse, table, preferred_element_type=f32) + jnp.dot(
                fine, table, preferred_element_type=f32
            )
            ref = ((keep, to_partner), (to_sib, to_diag))[source][part]
            ref[...] = total.astype(ref.dtype)


def combine(where, info, sib_info, returned, chunk):
    half = returned.shape[2] // 2
    per_half = 2
    whole = lambda i, w: (0, 0)
    shapes = [jax.ShapeDtypeStruct((MOE_DEV, half), t) for t in (f32, bf16, bf16, bf16)]
    return pl.pallas_call(
        combine_kernel,
        grid_spec=pltpu.PrefetchScalarGridSpec(
            num_scalar_prefetch=1,
            grid=(1,),
            in_specs=[
                pl.BlockSpec((MOE_DEV, 4), lambda i, w: (w[0] * per_half + chunk, 0)),
                pl.BlockSpec((MOE_DEV, 4), lambda i, w: (w[0] * per_half + chunk, 0)),
                pl.BlockSpec(returned.shape, lambda i, w: (0, 0, 0)),
            ],
            out_specs=[pl.BlockSpec((MOE_DEV, half), whole)] * 4,
        ),
        out_shape=shapes,
        cost_estimate=pl.CostEstimate(
            flops=4 << 30, bytes_accessed=4 << 20, transcendentals=0
        ),
        name="combine",
    )(where, info, sib_info, returned)


def conv_rows(conv_value, conv_gate, conv_taps, conv_gain, conv_bias):
    gated_rows = (
        conv_value.astype(f32) * jax.nn.sigmoid(conv_gate.astype(f32))
    ).astype(bf16)
    reach_back = conv_taps.shape[0] - 1
    length = gated_rows.shape[0]
    count = lax.axis_size(EP_TP)
    earlier = lax.ppermute(
        gated_rows[length - reach_back :], EP_TP, [(k, k + 1) for k in range(count - 1)]
    )
    extended = jnp.concatenate([earlier, gated_rows], axis=0)
    mixed = jnp.zeros(gated_rows.shape, f32)
    for lag in range(reach_back + 1):
        window = lax.slice_in_dim(extended, reach_back - lag, reach_back - lag + length, axis=0)
        mixed = mixed + conv_taps[lag] * window.astype(f32)
    center = mixed - jnp.mean(mixed, axis=-1, keepdims=True)
    spread = jnp.mean(center * center, axis=-1, keepdims=True)
    return jax.nn.silu(center * lax.rsqrt(spread + epsilon) * conv_gain + conv_bias).astype(bf16)


def on_device(
    conv_value,
    conv_gate,
    conv_taps,
    conv_gain,
    conv_bias,
    conv_projection,
    expert_input,
    expert_gain,
    route_experts,
    group_gate,
    expert_gate,
    gate_weight,
    up_weight,
    down_weight,
):
    core, x = lax.axis_index("ep_2"), lax.axis_index("tp")
    place = (x - core) % 4

    def half_of(which_core):
        spot = (x - which_core) % 4
        return ((spot == 1) | (spot == 2)).astype(jnp.int32)

    half, sib_half = half_of(core), half_of(1 - core)
    where = jnp.stack([half, core]).astype(jnp.int32)
    rows_half = expert_input.shape[0] // 2

    gate_own, up_own, down_own = gate_weight[0], up_weight[0], down_weight[0]

    outgoing = lax.dynamic_slice_in_dim(expert_input, sib_half * rows_half, rows_half, 0)
    share = group_gate[:, None] * expert_gate / jnp.sum(expert_gate, axis=1, keepdims=True)
    info = jnp.concatenate([route_experts.astype(f32), share], axis=1)
    sib_rows = swapped(outgoing, other_core)
    sib_info = swapped(info, other_core)
    gate_part = swapped(gate_own, weight_partner)
    up_part = swapped(up_own, weight_partner)
    gain = expert_gain[None]

    sends = [
        dispatch(where, expert_input, sib_rows, info, sib_info, gain, k) for k in range(CHUNKS)
    ]
    arrived = [
        lax.all_to_all(s, CHIPS, split_axis=0, concat_axis=0, tiled=True) for s in sends
    ]

    conv_value, conv_gate, _ = lax.optimization_barrier((conv_value, conv_gate, sends[0]))
    activated = conv_rows(conv_value, conv_gate, conv_taps, conv_gain, conv_bias)
    down_part = swapped(down_own, weight_partner)

    hidden_order = [place, place ^ 1, 3 - place, (3 - place) ^ 1]
    quarter = down_own.shape[0] // 4

    def ordered(matrix):
        return jnp.concatenate(
            [
                lax.dynamic_slice_in_dim(matrix, (p + core) % 4 * quarter, quarter, 0)
                for p in hidden_order
            ],
            axis=0,
        )

    down_all = jnp.concatenate([ordered(down_own), ordered(down_part)], axis=1)
    near, far = down_all[: 2 * quarter], down_all[2 * quarter :]

    pieces = []
    for k in range(CHUNKS):
        tokens = arrived[k].reshape(-1, arrived[k].shape[2])
        parts = []
        for gate_matrix, up_matrix in ((gate_own, up_own), (gate_part, up_part)):
            gate_out = jnp.dot(tokens, gate_matrix, preferred_element_type=f32)
            up_out = jnp.dot(tokens, up_matrix, preferred_element_type=f32)
            parts.append((jax.nn.silu(gate_out) * up_out).astype(bf16))
        hidden = jnp.concatenate(parts, axis=1)
        other = swapped(hidden, hidden_partner)
        summed = jnp.dot(hidden, near, preferred_element_type=f32)
        summed = summed + jnp.dot(other, far, preferred_element_type=f32)
        result = summed.astype(bf16).reshape(PLANES, 2 * CAP, -1)
        returned = lax.all_to_all(result, CHIPS, split_axis=0, concat_axis=0, tiled=True)
        keep, to_partner, to_sib, to_diag = combine(where, info, sib_info, returned, k)
        from_partner = swapped(to_partner, weight_partner)
        from_sib = swapped(to_sib, other_core)
        from_diag = swapped(to_diag, diagonal)
        mine = jnp.stack([keep, from_partner.astype(f32)])
        mine = jnp.where(half == 0, mine, mine[::-1])
        theirs = jnp.stack([from_sib.astype(f32), from_diag.astype(f32)])
        theirs = jnp.where(sib_half == 0, theirs, theirs[::-1])
        pieces.append((mine + theirs).astype(bf16))
    expert_out = jnp.stack(pieces, axis=1).reshape(expert_input.shape[0], -1)

    rows = activated.shape[0]
    middle = rows // 2
    right = [(k, (k + 1) % 4) for k in range(4)]
    left = [(k, (k - 1) % 4) for k in range(4)]
    from_left = lax.ppermute(activated, "tp", right)
    from_right = lax.ppermute(activated, "tp", left)
    far_top = lax.ppermute(from_left[:middle], "tp", right)
    far_bottom = lax.ppermute(from_right[middle:], "tp", left)
    conv_out = jnp.zeros((4 * rows, conv_projection.shape[1]), bf16)
    for block, offset, start in (
        (activated, 0, 0),
        (from_left, 3, 0),
        (from_right, 1, 0),
        (far_top, 2, 0),
        (far_bottom, 2, middle),
    ):
        product = jnp.dot(block, conv_projection, preferred_element_type=f32).astype(bf16)
        conv_out = lax.dynamic_update_slice_in_dim(
            conv_out, product, (x + offset) % 4 * rows + start, 0
        )
    return (conv_out, expert_out)


def solution(mesh):
    finer = Mesh(mesh.devices.reshape(4, 4, 2, mesh.shape["tp"]), EP_TP)
    in_specs = (
        P(EP_TP, None),
        P(EP_TP, None),
        P(),
        P(),
        P(),
        P(None, "tp"),
        P(EP, None),
        P(),
        P(EP, None),
        P(EP),
        P(EP, None),
        P(EP, None, "tp"),
        P(EP, None, "tp"),
        P(EP, None, "tp"),
    )
    out_specs = (P(EP, "tp"), P(EP, "tp"))
    return jax.shard_map(
        on_device, mesh=finer, in_specs=in_specs, out_specs=out_specs, check_vma=False
    )
```

time: 447 us -> 272 us (0.61)
  waiting for transfers between devices: 229 us -> 74.7 us
  blocking collectives: 69 us -> 0 us
  starting transfers between devices: 10.5 us -> 44.9 us
  local copies, waits for them, and re-layouts: 47.9 us -> 13.6 us
  Pallas kernels: 0 us -> 21.6 us
  matrix products: 34.9 us -> 55.2 us
  other arithmetic: 40.1 us -> 55.4 us
  between operations: 14.1 us -> 1.76 us
    all_gather x4 -> x0, waiting for transfers between devices: 224 us -> none  [the longest x1 151 us: on_device(): hidden_arrived = lax.all_gather(arrived, 'tp', axis=0, tiled=True)]
    all_to_all x2 -> x0, blocking collectives: 69 us -> none  [the longest x1 60.3 us: on_device(): lax.all_to_all(outgoing, EP, split_axis=1, concat_axis=2, tiled=True)]
    all_to_all x1 -> x4, waiting for transfers between devices: 0.01 us -> 46.9 us  [the longest x2 28.3 us: on_device(): lax.all_to_all(s, CHIPS, split_axis=0, concat_axis=0, tiled=True)]
    concatenate x1 -> x4, other arithmetic: 1.97 us -> 34.1 us  [the longest x1 34 us: on_device(): down_all = jnp.concatenate([ordered(down_own), ordered(down_part)], axis=1)]
    gather x4 -> x0, local copies, waits for them, and re-layouts: 30.4 us -> none  [the longest x2 17.4 us: take_rows(): return jnp.take(normed, jnp.maximum(source, 0), axis=0)]
    ppermute x1 -> x18, waiting for transfers between devices: 4.51 us -> 27.7 us  [the longest x13 27.7 us: swapped(): return lax.ppermute(value, CORE_TP, ring_pairs(move))]
    pallas_call x0 -> x4, Pallas kernels: none -> 21.6 us  [the longest x2 12.2 us: dispatch(): pl.pallas_call(dispatch_kernel, grid_spec=pltpu.PrefetchScalarGridSpec(nu...]
    dot_general x5 -> x17, matrix products: 34.9 us -> 55.2 us  [the longest x4 16.2 us: on_device(): gate_out = jnp.dot(tokens, gate_matrix, preferred_element_type=f32)]
  transfers between devices with their start and end apart: 6 -> 22, of which waited for: 5 -> 7; matrix products, arithmetic and copies ran while one was open for 11% -> 44% of each run, Pallas kernels for 0% -> 6%
where the time goes in v1:
time: 272 us; the launch traced here: 267 us
  waiting for transfers between devices  74.7 us (27%)
  other arithmetic  55.4 us (20%)
  matrix products  55.2 us (20%)
  starting transfers between devices  44.9 us (17%)
  Pallas kernels  21.6 us (8%)
  local copies, waits for them, and re-layouts  13.6 us (5%)
    concatenate x1, other arithmetic, on_device(): down_all = jnp.concatenate([ordered(down_own), ordered(down_part)], axis=1)  34 us
    all_to_all x2, waiting for transfers between devices, on_device(): lax.all_to_all(s, CHIPS, split_axis=0, concat_axis=0, tiled=True)  28.3 us
    ppermute x13, waiting for transfers between devices, swapped(): return lax.ppermute(value, CORE_TP, ring_pairs(move))  27.7 us
    all_to_all x2, waiting for transfers between devices, on_device(): lax.all_to_all(result, CHIPS, split_axis=0, concat_axis=0, tiled=True)  18.6 us
    dot_general x4, matrix products, on_device(): gate_out = jnp.dot(tokens, gate_matrix, preferred_element_type=f32)  16.2 us
    dot_general x5, matrix products, on_device(): jnp.dot(block, conv_projection, preferred_element_type=f32).astype(bf16)  15.5 us
    dot_general x4, matrix products, on_device(): up_out = jnp.dot(tokens, up_matrix, preferred_element_type=f32)  15.5 us
    reduce_sum x1, other arithmetic, conv_rows(): center = mixed - jnp.mean(mixed, axis=-1, keepdims=True)  14.5 us
  transfers between devices with their start and end apart: 22, of which 7 were waited for; matrix products, arithmetic and copies ran while one was open for 44% of the time, Pallas kernels for 6%

profile of v1, /device:TPU:1, one launch (start us, length us, event | category | flops | bytes accessed | tf_op | source)
XLA Modules:
  0.0 267.1 jit_solution(4925237247294090640)
XLA Ops:
  0.7 1.7 constant_dynamic-slice_fusion.4
  2.4 1.5 collective-permute-start
  4.0 0.1 copy.26.own_info
  4.1 0.1 collective-permute-start.1
  4.2 0.7 pad_add_fusion.where
  4.9 3.2 %collective-permute-done.1.sib_info = f32[512,4]{1,0:T(8,128)S(1)} collective-permute-done((f32[512,4]{1,0:T(8,128)S(1)}, f32[512,4]{1,0:T(8,128)S(1)}, u32[]{:S(2)}, u32[]{:S(2)}) %collective-permute-start.1) | collective-permute-done | bytes 8224 | tf_op jit(solution)/shard_map/ppermute | solution.py:52
  8.1 0.7 copy-done.18
  8.8 6.0 %dispatch.2 = bf16[16,32,4096]{2,1,0:T(8,128)(2,1)} custom-call(s32[2]{0:T(128)} %pad_add_fusion.where, bf16[512,4096]{1,0:T(8,128)(2,1)} %own_ref.3, bf16[256,4096]{1,0:T(8,128)(2,1)} %collective-permute-done.sib_ref, f32[512,4]{1,0:T(8,128)} %copy-done.6, f32[512,4]{1,0:T(8,128)} %copy-done.18, f32[1,4096]{1,0:T(1,128)} %bitcast.142), custom_call_target="tpu_custom_call" | custom-call | flops 4294967296 | bytes 8388608 | tf_op jit(solution)/shard_map/dispatch/pallas_call | solution.py:108
  14.8 7.9 %all-to-all-start = ((bf16[16,32,4096]{2,1,0:T(8,128)(2,1)}), bf16[16,32,4096]{2,1,0:T(8,128)(2,1)}, u32[]{:S(2)}, u32[]{:S(2)}) async-start(bf16[16,32,4096]{2,1,0:T(8,128)(2,1)} %dispatch.2), calls=%async_computation | async-start | bytes 8388608 | tf_op jit(solution)/shard_map/all_to_all | solution.py:242
  22.7 2.6 collective-permute-start.9
  25.3 0.2 collective-permute-start.7
  25.5 2.5 collective-permute-start.8
  28.0 1.7 dynamic-slice_bitcast_fusion.3
  29.8 0.1 fusion.65
  29.9 2.3 multiply_convert_fusion.1
  32.2 2.4 collective-permute-start.2
  34.6 16.3 %collective-permute-done.9 = bf16[1024,1024]{1,0:T(8,128)(2,1)} collective-permute-done((bf16[1024,1024]{1,0:T(8,128)(2,1)}, bf16[1024,1024]{1,0:T(8,128)(2,1)}, u32[]{:S(2)}, u32[]{:S(2)}) %collective-permute-start.9) | collective-permute-done | bytes 2097184 | tf_op jit(solution)/shard_map/ppermute | solution.py:52
  50.9 1.7 constant_dynamic-slice_fusion.3
  52.6 34.0 %maximum_maximum_fusion = bf16[1024,2048]{1,0:T(8,128)(2,1)} fusion(bf16[256,1024]{1,0:T(8,128)(2,1)S(1)} %get-tuple-element.29, bf16[256,1024]{1,0:T(8,128)(2,1)S(1)} %get-tuple-element.30, bf16[256,1024]{1,0:T(8,128)(2,1)S(1)} %get-tuple-element.31, bf16[256,1024]{1,0:T(8,128)(2,1)S(1)} %get-tuple-element.28, bf16[256,1024]{1,0:T(8,128)(2,1)S(1)} %get-tuple-element.27, ...), kind=kLoop, calls=%fused_computation.29 | loop fusion | flops 33554432 | bytes 8388608 | tf_op jit(solution)/shard_map/concatenate | solution.py:261
  86.6 6.2 %dispatch.3 = bf16[16,32,4096]{2,1,0:T(8,128)(2,1)} custom-call(s32[2]{0:T(128)} %pad_add_fusion.where, bf16[512,4096]{1,0:T(8,128)(2,1)} %own_ref.3, bf16[256,4096]{1,0:T(8,128)(2,1)} %collective-permute-done.sib_ref, f32[512,4]{1,0:T(8,128)} %copy-done.6, f32[512,4]{1,0:T(8,128)} %copy-done.18, f32[1,4096]{1,0:T(1,128)} %bitcast.143), custom_call_target="tpu_custom_call" | custom-call | flops 4294967296 | bytes 8388608 | tf_op jit(solution)/shard_map/dispatch/pallas_call | solution.py:108
  92.8 6.5 %all-to-all-start.2 = ((bf16[16,32,4096]{2,1,0:T(8,128)(2,1)}), bf16[16,32,4096]{2,1,0:T(8,128)(2,1)}, u32[]{:S(2)}, u32[]{:S(2)}) async-start(bf16[16,32,4096]{2,1,0:T(8,128)(2,1)} %dispatch.3), calls=%async_computation.2 | async-start | bytes 8388608 | tf_op jit(solution)/shard_map/all_to_all | solution.py:242
  99.4 14.5 %fusion.64 = (f32[384]{0:T(512)S(1)}, f32[384,2048]{1,0:T(8,128)S(1)}) fusion(bf16[384,2048]{1,0:T(8,128)(2,1)S(1)} %multiply_convert_fusion.1, bf16[30,2048]{1,0:T(8,128)(2,1)S(1)} %collective-permute-done.2, f32[2048]{0:T(1024)S(1)} %bitcast.119, f32[2048]{0:T(1024)S(1)} %bitcast.120, f32[2048]{0:T(1024)S(1)} %bitcast.122, f32[2048]{0:T(1024)S(1)} %bitcast.123, ...), kind=kLoop, calls=%fused_computation.135 | loop fusion | flops 143916672 | bytes 5096960 | tf_op jit(solution)/shard_map/reduce_sum | solution.py:195
  113.9 0.5 multiply_reduce_fusion
  114.3 2.5 multiply_convert_fusion
  116.8 2.7 %collective-permute-start.4 = (bf16[384,2048]{1,0:T(8,128)(2,1)}, bf16[384,2048]{1,0:T(8,128)(2,1)}, u32[]{:S(2)}, u32[]{:S(2)}) collective-permute-start(bf16[384,2048]{1,0:T(8,128)(2,1)} %multiply_convert_fusion), channel_id=1, source_target_pairs={{0,3},{1,0},{2,1},{3,2},{4,7},{5,4},{6,5},{7,6},{8,11},{9,8},{10,9... | collective-permute-start | bytes 4718600 | tf_op jit(solution)/shard_map/ppermute | solution.py:294
  119.5 3.5 %fusion.62 = f32[512,256]{0,1:T(8,128)S(1)} fusion(bf16[512,4096]{1,0:T(8,128)(2,1)} %bitcast.34, bf16[1,4096,256]{2,1,0:T(8,128)(2,1)S(1)} %copy-done.15), kind=kOutput, calls=%fused_computation.133 | convolution fusion | flops 1073741824 | bytes 6815744 | tf_op jit(solution)/shard_map/dot_general | solution.py:269
  123.0 4.3 %fusion.67 = f32[512,256]{0,1:T(8,128)S(1)} fusion(bf16[512,4096]{1,0:T(8,128)(2,1)} %bitcast.34, bf16[4096,256]{1,0:T(8,128)(2,1)} %collective-permute-done.7), kind=kOutput, calls=%fused_computation.138 | convolution fusion | flops 1073741824 | bytes 6815744 | tf_op jit(solution)/shard_map/dot_general | solution.py:269
  127.3 3.5 %multiply_convert_fusion.5 = bf16[512,256]{0,1:T(8,128)(2,1)S(1)} fusion(f32[512,256]{0,1:T(8,128)S(1)} %fusion.62, bf16[512,4096]{1,0:T(8,128)(2,1)} %bitcast.34, bf16[1,4096,256]{2,1,0:T(8,128)(2,1)S(1)} %copy-done.16), kind=kOutput, calls=%fused_computation.114 | convolution fusion | flops 1074528256 | bytes 7077888 | tf_op jit(solution)/shard_map/dot_general | solution.py:270
  130.9 4.2 %multiply_convert_fusion.4 = bf16[512,256]{0,1:T(8,128)(2,1)S(1)} fusion(f32[512,256]{0,1:T(8,128)S(1)} %fusion.67, bf16[512,4096]{1,0:T(8,128)(2,1)} %bitcast.34, bf16[4096,256]{1,0:T(8,128)(2,1)} %collective-permute-done.8), kind=kOutput, calls=%fused_computation.113 | convolution fusion | flops 1074528256 | bytes 7077888 | tf_op jit(solution)/shard_map/dot_general | solution.py:270
  135.1 0.3 collective-permute-start.10
  135.4 28.3 %all-to-all-done.2 = bf16[16,32,4096]{2,1,0:T(8,128)(2,1)} async-done(((bf16[16,32,4096]{2,1,0:T(8,128)(2,1)}), bf16[16,32,4096]{2,1,0:T(8,128)(2,1)}, u32[]{:S(2)}, u32[]{:S(2)}) %all-to-all-start.2) | async-done | bytes 4194336 | tf_op jit(solution)/shard_map/all_to_all | solution.py:242
  163.7 4.2 %fusion.60 = f32[512,256]{0,1:T(8,128)S(1)} fusion(bf16[512,4096]{1,0:T(8,128)(2,1)} %bitcast.48, bf16[1,4096,256]{2,1,0:T(8,128)(2,1)} %param.25), kind=kOutput, calls=%fused_computation.131 | convolution fusion | flops 1073741824 | bytes 6815744 | tf_op jit(solution)/shard_map/dot_general | solution.py:269
  167.9 4.3 %fusion.68 = f32[512,256]{0,1:T(8,128)S(1)} fusion(bf16[512,4096]{1,0:T(8,128)(2,1)} %bitcast.48, bf16[4096,256]{1,0:T(8,128)(2,1)} %collective-permute-done.7), kind=kOutput, calls=%fused_computation.139 | convolution fusion | flops 1073741824 | bytes 6815744 | tf_op jit(solution)/shard_map/dot_general | solution.py:269
  172.2 3.7 %multiply_convert_fusion.3 = bf16[512,256]{0,1:T(8,128)(2,1)S(1)} fusion(f32[512,256]{0,1:T(8,128)S(1)} %fusion.60, bf16[512,4096]{1,0:T(8,128)(2,1)} %bitcast.48, bf16[1,4096,256]{2,1,0:T(8,128)(2,1)S(1)} %copy-done.17), kind=kOutput, calls=%fused_computation.108 | convolution fusion | flops 1074528256 | bytes 7077888 | tf_op jit(solution)/shard_map/dot_general | solution.py:270
  175.9 1.3 fusion.2
  177.2 2.7 %add_convert_fusion.1 = bf16[512,2048]{1,0:T(8,128)(2,1)} fusion(f32[512,2048]{1,0:T(8,128)S(1)} %fusion.2, bf16[1024,2048]{1,0:T(8,128)(2,1)S(1)} %copy-done, bf16[512,256]{0,1:T(8,128)(2,1)S(1)} %multiply_convert_fusion.4, bf16[512,256]{0,1:T(8,128)(2,1)S(1)} %multiply_convert_fusion.5), kind=kOutput, calls=%fused_computation.31 | convolution fusion | flops 1076887552 | bytes 8912896 | tf_op jit(solution)/shard_map/dot_general | solution.py:274
  179.9 4.4 %all-to-all-start.1 = ((bf16[16,32,2048]{2,1,0:T(8,128)(2,1)}), bf16[16,32,2048]{2,1,0:T(8,128)(2,1)}, u32[]{:S(2)}, u32[]{:S(2)}) async-start(bf16[16,32,2048]{2,1,0:T(8,128)(2,1)} %bitcast.42), calls=%async_computation.1 | async-start | bytes 4194304 | tf_op jit(solution)/shard_map/all_to_all | solution.py:277
  184.4 4.2 %multiply_convert_fusion.2 = bf16[512,256]{0,1:T(8,128)(2,1)S(1)} fusion(f32[512,256]{0,1:T(8,128)S(1)} %fusion.68, bf16[512,4096]{1,0:T(8,128)(2,1)} %bitcast.48, bf16[4096,256]{1,0:T(8,128)(2,1)} %collective-permute-done.8), kind=kOutput, calls=%fused_computation.107 | convolution fusion | flops 1074528256 | bytes 7077888 | tf_op jit(solution)/shard_map/dot_general | solution.py:270
  188.7 0.4 broadcast_in_dim.4
  189.1 1.6 copy-done.13
  190.7 3.4 %fusion.43 = bf16[1536,1024]{1,0:T(8,128)(2,1)S(1)} fusion(bf16[1536,1024]{1,0:T(8,128)(2,1)S(1)} %broadcast_in_dim.4, s32[]{:T(128)S(6)} %select_n.112, bf16[384,2048]{1,0:T(8,128)(2,1)} %multiply_convert_fusion, bf16[2048,1024]{1,0:T(8,128)(2,1)S(1)} %copy-done.13), kind=kOutput, calls=%fused_computation.89 | convolution fusion | flops 1611005952 | bytes 6553604 | tf_op jit(solution)/shard_map/dot_general | solution.py:305
  194.1 2.1 slice.323
  196.2 2.1 slice.324
  198.4 2.9 %collective-permute-start.6 = (bf16[192,2048]{1,0:T(8,128)(2,1)}, bf16[192,2048]{1,0:T(8,128)(2,1)}, u32[]{:S(2)}, u32[]{:S(2)}) collective-permute-start(bf16[192,2048]{1,0:T(8,128)(2,1)} %slice.324), channel_id=1, source_target_pairs={{0,3},{1,0},{2,1},{3,2},{4,7},{5,4},{6,5},{7,6},{8,11},{9,8},{10,9... | collective-permute-start | bytes 2359304 | tf_op jit(solution)/shard_map/ppermute | solution.py:296
  201.3 1.3 fusion
  202.6 2.6 add_convert_fusion
  205.2 10.4 %all-to-all-done.1.result_ref = bf16[16,32,2048]{2,1,0:T(8,128)(2,1)} async-done(((bf16[16,32,2048]{2,1,0:T(8,128)(2,1)}), bf16[16,32,2048]{2,1,0:T(8,128)(2,1)}, u32[]{:S(2)}, u32[]{:S(2)}) %all-to-all-start.1) | async-done | bytes 2097184 | tf_op jit(solution)/shard_map/all_to_all | solution.py:277
  215.6 4.4 %all-to-all-start.3 = ((bf16[16,32,2048]{2,1,0:T(8,128)(2,1)}), bf16[16,32,2048]{2,1,0:T(8,128)(2,1)}, u32[]{:S(2)}, u32[]{:S(2)}) async-start(bf16[16,32,2048]{2,1,0:T(8,128)(2,1)} %bitcast.49), calls=%async_computation.3 | async-start | bytes 4194304 | tf_op jit(solution)/shard_map/all_to_all | solution.py:277
  220.0 4.6 %fusion.42 = bf16[1536,1024]{1,0:T(8,128)(2,1)S(1)} fusion(bf16[1536,1024]{1,0:T(8,128)(2,1)S(1)} %fusion.43, s32[]{:T(128)S(6)} %select_n.114, bf16[384,2048]{1,0:T(8,128)(2,1)} %collective-permute-done.3, bf16[2048,1024]{1,0:T(8,128)(2,1)} %param.19), kind=kOutput, calls=%fused_computation.87 | convolution fusion | flops 1611005952 | bytes 6553604 | tf_op jit(solution)/shard_map/dot_general | solution.py:305
  224.6 3.2 %fusion.41 = bf16[1536,1024]{1,0:T(8,128)(2,1)S(1)} fusion(bf16[1536,1024]{1,0:T(8,128)(2,1)S(1)} %fusion.42, s32[]{:T(128)S(6)} %select_n.116, bf16[384,2048]{1,0:T(8,128)(2,1)} %collective-permute-done.4, bf16[2048,1024]{1,0:T(8,128)(2,1)S(1)} %copy-done.14), kind=kOutput, calls=%fused_computation.85 | convolution fusion | flops 1611005952 | bytes 6553604 | tf_op jit(solution)/shard_map/dot_general | solution.py:305
  227.9 2.2 fusion.45
  230.1 2.2 fusion.44
  232.2 4.9 %combine.2 = (f32[128,1024]{1,0:T(8,128)}, bf16[128,1024]{1,0:T(8,128)(2,1)}, bf16[128,1024]{1,0:T(8,128)(2,1)}, bf16[128,1024]{1,0:T(8,128)(2,1)}) custom-call(s32[2]{0:T(128)} %pad_add_fusion.where, f32[512,4]{1,0:T(8,128)} %copy-done.6, f32[512,4]{1,0:T(8,128)} %copy-done.18, bf16[16,32,2048]{2,1,0:T(8,128)(2,1)} %all-to-all-done.1.result_ref), custom_call_target="tpu_custom_call" | custom-call | flops 4294967296 | bytes 4194304 | tf_op jit(solution)/shard_map/combine/pallas_call | solution.py:160
  237.1 1.8 collective-permute-start.12
  238.9 1.3 collective-permute-start.13
  240.2 8.2 %all-to-all-done.3.result_ref = bf16[16,32,2048]{2,1,0:T(8,128)(2,1)} async-done(((bf16[16,32,2048]{2,1,0:T(8,128)(2,1)}), bf16[16,32,2048]{2,1,0:T(8,128)(2,1)}, u32[]{:S(2)}, u32[]{:S(2)}) %all-to-all-start.3) | async-done | bytes 2097184 | tf_op jit(solution)/shard_map/all_to_all | solution.py:277
  248.4 4.5 %combine.3 = (f32[128,1024]{1,0:T(8,128)}, bf16[128,1024]{1,0:T(8,128)(2,1)}, bf16[128,1024]{1,0:T(8,128)(2,1)}, bf16[128,1024]{1,0:T(8,128)(2,1)}) custom-call(s32[2]{0:T(128)} %pad_add_fusion.where, f32[512,4]{1,0:T(8,128)} %copy-done.6, f32[512,4]{1,0:T(8,128)} %copy-done.18, bf16[16,32,2048]{2,1,0:T(8,128)(2,1)} %all-to-all-done.3.result_ref), custom_call_target="tpu_custom_call" | custom-call | flops 4294967296 | bytes 4194304 | tf_op jit(solution)/shard_map/combine/pallas_call | solution.py:160
  253.0 3.3 %collective-permute-start.16 = (bf16[128,1024]{1,0:T(8,128)(2,1)}, bf16[128,1024]{1,0:T(8,128)(2,1)S(1)}, u32[]{:S(2)}, u32[]{:S(2)}) collective-permute-start(bf16[128,1024]{1,0:T(8,128)(2,1)} %get-tuple-element.20), channel_id=1, source_target_pairs={{0,4},{1,5},{2,6},{3,7},{4,0},{5,1},{6,2},{7,3},{8,12},{9,13},{10,... | collective-permute-start | bytes 786440 | tf_op jit(solution)/shard_map/ppermute | solution.py:52
  256.5 3.1 %collective-permute-done.15 = bf16[128,1024]{1,0:T(8,128)(2,1)S(1)} collective-permute-done((bf16[128,1024]{1,0:T(8,128)(2,1)}, bf16[128,1024]{1,0:T(8,128)(2,1)S(1)}, u32[]{:S(2)}, u32[]{:S(2)}) %collective-permute-start.15) | collective-permute-done | bytes 262176 | tf_op jit(solution)/shard_map/ppermute | solution.py:52
  259.9 5.1 %collective-permute-done.17 = bf16[128,1024]{1,0:T(8,128)(2,1)S(1)} collective-permute-done((bf16[128,1024]{1,0:T(8,128)(2,1)}, bf16[128,1024]{1,0:T(8,128)(2,1)S(1)}, u32[]{:S(2)}, u32[]{:S(2)}) %collective-permute-start.17) | collective-permute-done | bytes 262176 | tf_op jit(solution)/shard_map/ppermute | solution.py:52
  265.1 0.2 fusion.51
  265.3 0.2 fusion.50
  265.5 0.1 pad_maximum_fusion.3
  265.6 1.0 copy.30
  (73 shorter events, 0.8 us)
Async XLA Ops:
  0.6 3.3 %copy-start.11 = (s32[512,2]{0,1:T(2,128)S(1)}, s32[512,2]{0,1:T(2,128)}, u32[]{:S(2)}) copy-start(s32[512,2]{0,1:T(2,128)} %param.22) | copy-start | bytes 12292
  0.6 3.3 %copy-start.8 = (f32[512,2]{0,1:T(2,128)S(1)}, f32[512,2]{0,1:T(2,128)}, u32[]{:S(2)}) copy-start(f32[512,2]{0,1:T(2,128)} %param.24) | copy-start | bytes 12292
  0.7 3.3 %copy-start.12 = (f32[512]{0:T(512)S(1)}, f32[512]{0:T(512)}, u32[]{:S(2)}) copy-start(f32[512]{0:T(512)} %param.23) | copy-start | bytes 6148
  2.4 5.6 %collective-permute-start = (bf16[256,4096]{1,0:T(8,128)(2,1)S(1)}, bf16[256,4096]{1,0:T(8,128)(2,1)}, u32[]{:S(2)}, u32[]{:S(2)}) collective-permute-start(bf16[256,4096]{1,0:T(8,128)(2,1)S(1)} %constant_dynamic-slice_fusion.4), channel_id=1, source_target_pairs={{0,4},{1,5},{2,6},{3,7},{4,0},{5,1},{6,2},{7,3},{8,12},{9,13},{10,... | collective-permute-start | bytes 6291464 | tf_op jit(solution)/shard_map/ppermute | solution.py:52
  4.1 3.9 %copy-start.6 = (f32[512,4]{1,0:T(8,128)}, f32[512,4]{1,0:T(8,128)S(1)}, u32[]{:S(2)}) copy-start(f32[512,4]{1,0:T(8,128)S(1)} %copy.26.own_info) | copy-start | bytes 24580
  4.1 3.9 %collective-permute-start.1 = (f32[512,4]{1,0:T(8,128)S(1)}, f32[512,4]{1,0:T(8,128)S(1)}, u32[]{:S(2)}, u32[]{:S(2)}) collective-permute-start(f32[512,4]{1,0:T(8,128)S(1)} %copy.26.own_info), channel_id=1, source_target_pairs={{0,4},{1,5},{2,6},{3,7},{4,0},{5,1},{6,2},{7,3},{8,12},{9,13},{10,... | collective-permute-start | bytes 24584 | tf_op jit(solution)/shard_map/ppermute | solution.py:52
  8.0 0.7 copy-start.18
  14.8 78.1 %all-to-all-start = ((bf16[16,32,4096]{2,1,0:T(8,128)(2,1)}), bf16[16,32,4096]{2,1,0:T(8,128)(2,1)}, u32[]{:S(2)}, u32[]{:S(2)}) async-start(bf16[16,32,4096]{2,1,0:T(8,128)(2,1)} %dispatch.2), calls=%async_computation | async-start | bytes 8388608 | tf_op jit(solution)/shard_map/all_to_all | solution.py:242
  22.7 7.0 %copy-start.7 = (f32[31,2048]{1,0:T(8,128)S(1)}, f32[31,2048]{1,0:T(8,128)}, u32[]{:S(2)}) copy-start(f32[31,2048]{1,0:T(8,128)} %param.16) | copy-start | bytes 761860
  22.7 7.2 %copy-start.3 = (bf16[384,2048]{1,0:T(8,128)(2,1)S(1)}, bf16[384,2048]{1,0:T(8,128)(2,1)}, u32[]{:S(2)}) copy-start(bf16[384,2048]{1,0:T(8,128)(2,1)} %param.15) | copy-start | bytes 4718596
  22.7 28.2 %collective-permute-start.9 = (bf16[1024,1024]{1,0:T(8,128)(2,1)}, bf16[1024,1024]{1,0:T(8,128)(2,1)}, u32[]{:S(2)}, u32[]{:S(2)}) collective-permute-start(bf16[1024,1024]{1,0:T(8,128)(2,1)} %bitcast.41), channel_id=1, source_target_pairs={{0,1},{1,0},{2,3},{3,2},{4,7},{5,6},{6,5},{7,4},{8,9},{9,8},{10,11... | collective-permute-start | bytes 6291464 | tf_op jit(solution)/shard_map/ppermute | solution.py:52
  25.3 97.7 %collective-permute-start.7 = (bf16[4096,256]{1,0:T(8,128)(2,1)}, bf16[4096,256]{1,0:T(8,128)(2,1)}, u32[]{:S(2)}, u32[]{:S(2)}) collective-permute-start(bf16[4096,256]{1,0:T(8,128)(2,1)} %bitcast.140), channel_id=1, source_target_pairs={{0,1},{1,0},{2,3},{3,2},{4,7},{5,6},{6,5},{7,4},{8,9},{9,8},{10,11... | collective-permute-start | bytes 6291464 | tf_op jit(solution)/shard_map/ppermute | solution.py:52
  25.5 105.4 %collective-permute-start.8 = (bf16[4096,256]{1,0:T(8,128)(2,1)}, bf16[4096,256]{1,0:T(8,128)(2,1)}, u32[]{:S(2)}, u32[]{:S(2)}) collective-permute-start(bf16[4096,256]{1,0:T(8,128)(2,1)} %bitcast.141), channel_id=1, source_target_pairs={{0,1},{1,0},{2,3},{3,2},{4,7},{5,6},{6,5},{7,4},{8,9},{9,8},{10,11... | collective-permute-start | bytes 6291464 | tf_op jit(solution)/shard_map/ppermute | solution.py:52
  32.2 67.1 %collective-permute-start.2 = (bf16[30,2048]{1,0:T(8,128)(2,1)S(1)}, bf16[30,2048]{1,0:T(8,128)(2,1)S(1)}, u32[]{:S(2)}, u32[]{:S(2)}) collective-permute-start(bf16[30,2048]{1,0:T(8,128)(2,1)S(1)} %slice.264), channel_id=1, source_target_pairs={{0,1},{1,2},{2,3},{3,4},{4,5},{5,6},{6,7},{7,8},{8,9},{9,10},{10,1... | collective-permute-start | bytes 368648 | tf_op jit(solution)/shard_map/ppermute | solution.py:187
  92.8 70.9 %all-to-all-start.2 = ((bf16[16,32,4096]{2,1,0:T(8,128)(2,1)}), bf16[16,32,4096]{2,1,0:T(8,128)(2,1)}, u32[]{:S(2)}, u32[]{:S(2)}) async-start(bf16[16,32,4096]{2,1,0:T(8,128)(2,1)} %dispatch.3), calls=%async_computation.2 | async-start | bytes 8388608 | tf_op jit(solution)/shard_map/all_to_all | solution.py:242
  99.4 15.0 %copy-start.9 = (f32[2048]{0:T(1024)S(1)}, f32[2048]{0:T(1024)}, u32[]{:S(2)}) copy-start(f32[2048]{0:T(1024)} %param.18) | copy-start | bytes 24580
  99.4 15.0 %copy-start.10 = (f32[2048]{0:T(1024)S(1)}, f32[2048]{0:T(1024)}, u32[]{:S(2)}) copy-start(f32[2048]{0:T(1024)} %param.17) | copy-start | bytes 24580
  114.3 5.2 %copy-start.15 = (bf16[1,4096,256]{2,1,0:T(8,128)(2,1)S(1)}, bf16[1,4096,256]{2,1,0:T(8,128)(2,1)}, u32[]{:S(2)}) copy-start(bf16[1,4096,256]{2,1,0:T(8,128)(2,1)} %param.25) | copy-start | bytes 6291460
  116.8 77.3 %collective-permute-start.3 = (bf16[384,2048]{1,0:T(8,128)(2,1)}, bf16[384,2048]{1,0:T(8,128)(2,1)}, u32[]{:S(2)}, u32[]{:S(2)}) collective-permute-start(bf16[384,2048]{1,0:T(8,128)(2,1)} %multiply_convert_fusion), channel_id=1, source_target_pairs={{0,1},{1,2},{2,3},{3,0},{4,5},{5,6},{6,7},{7,4},{8,9},{9,10},{10,1... | collective-permute-start | bytes 4718600 | tf_op jit(solution)/shard_map/ppermute | solution.py:293
  116.8 79.4 %collective-permute-start.4 = (bf16[384,2048]{1,0:T(8,128)(2,1)}, bf16[384,2048]{1,0:T(8,128)(2,1)}, u32[]{:S(2)}, u32[]{:S(2)}) collective-permute-start(bf16[384,2048]{1,0:T(8,128)(2,1)} %multiply_convert_fusion), channel_id=1, source_target_pairs={{0,3},{1,0},{2,1},{3,2},{4,7},{5,4},{6,5},{7,6},{8,11},{9,8},{10,9... | collective-permute-start | bytes 4718600 | tf_op jit(solution)/shard_map/ppermute | solution.py:294
  123.0 4.3 %copy-start.16 = (bf16[1,4096,256]{2,1,0:T(8,128)(2,1)S(1)}, bf16[1,4096,256]{2,1,0:T(8,128)(2,1)}, u32[]{:S(2)}) copy-start(bf16[1,4096,256]{2,1,0:T(8,128)(2,1)} %param.26) | copy-start | bytes 6291460
  135.1 40.8 %collective-permute-start.10 = (bf16[512,512]{0,1:T(8,128)(2,1)S(1)}, bf16[512,512]{0,1:T(8,128)(2,1)S(1)}, u32[]{:S(2)}, u32[]{:S(2)}) collective-permute-start(bf16[512,512]{0,1:T(8,128)(2,1)S(1)} %pad_maximum_fusion.4), channel_id=1, source_target_pairs={{0,3},{1,2},{2,1},{3,0},{4,5},{5,4},{6,7},{7,6},{8,11},{9,10},{10,... | collective-permute-start | bytes 1572872 | tf_op jit(solution)/shard_map/ppermute | solution.py:52
  167.9 4.3 %copy-start.17 = (bf16[1,4096,256]{2,1,0:T(8,128)(2,1)S(1)}, bf16[1,4096,256]{2,1,0:T(8,128)(2,1)}, u32[]{:S(2)}) copy-start(bf16[1,4096,256]{2,1,0:T(8,128)(2,1)} %param.26) | copy-start | bytes 6291460
  172.2 3.7 %copy-start = (bf16[1024,2048]{1,0:T(8,128)(2,1)S(1)}, bf16[1024,2048]{1,0:T(8,128)(2,1)}, u32[]{:S(2)}) copy-start(bf16[1024,2048]{1,0:T(8,128)(2,1)} %maximum_maximum_fusion) | copy-start | bytes 12582916
  179.9 35.6 %all-to-all-start.1 = ((bf16[16,32,2048]{2,1,0:T(8,128)(2,1)}), bf16[16,32,2048]{2,1,0:T(8,128)(2,1)}, u32[]{:S(2)}, u32[]{:S(2)}) async-start(bf16[16,32,2048]{2,1,0:T(8,128)(2,1)} %bitcast.42), calls=%async_computation.1 | async-start | bytes 4194304 | tf_op jit(solution)/shard_map/all_to_all | solution.py:277
  188.6 2.2 copy-start.13
  188.6 12.7 %collective-permute-start.14 = (bf16[512,512]{0,1:T(8,128)(2,1)S(1)}, bf16[512,512]{0,1:T(8,128)(2,1)S(1)}, u32[]{:S(2)}, u32[]{:S(2)}) collective-permute-start(bf16[512,512]{0,1:T(8,128)(2,1)S(1)} %pad_maximum_fusion.5), channel_id=1, source_target_pairs={{0,3},{1,2},{2,1},{3,0},{4,5},{5,4},{6,7},{7,6},{8,11},{9,10},{10,... | collective-permute-start | bytes 1572872 | tf_op jit(solution)/shard_map/ppermute | solution.py:52
  190.7 10.6 %copy-start.1 = (bf16[1024,2048]{1,0:T(8,128)(2,1)S(1)}, bf16[1024,2048]{1,0:T(8,128)(2,1)}, u32[]{:S(2)}) copy-start(bf16[1024,2048]{1,0:T(8,128)(2,1)} %maximum_maximum_fusion) | copy-start | bytes 12582916
  196.2 31.6 %collective-permute-start.5 = (bf16[192,2048]{1,0:T(8,128)(2,1)}, bf16[192,2048]{1,0:T(8,128)(2,1)}, u32[]{:S(2)}, u32[]{:S(2)}) collective-permute-start(bf16[192,2048]{1,0:T(8,128)(2,1)} %slice.323), channel_id=1, source_target_pairs={{0,1},{1,2},{2,3},{3,0},{4,5},{5,6},{6,7},{7,4},{8,9},{9,10},{10,1... | collective-permute-start | bytes 2359304 | tf_op jit(solution)/shard_map/ppermute | solution.py:295
  198.4 31.7 %collective-permute-start.6 = (bf16[192,2048]{1,0:T(8,128)(2,1)}, bf16[192,2048]{1,0:T(8,128)(2,1)}, u32[]{:S(2)}, u32[]{:S(2)}) collective-permute-start(bf16[192,2048]{1,0:T(8,128)(2,1)} %slice.324), channel_id=1, source_target_pairs={{0,3},{1,0},{2,1},{3,2},{4,7},{5,4},{6,5},{7,6},{8,11},{9,8},{10,9... | collective-permute-start | bytes 2359304 | tf_op jit(solution)/shard_map/ppermute | solution.py:296
  215.6 32.9 %all-to-all-start.3 = ((bf16[16,32,2048]{2,1,0:T(8,128)(2,1)}), bf16[16,32,2048]{2,1,0:T(8,128)(2,1)}, u32[]{:S(2)}, u32[]{:S(2)}) async-start(bf16[16,32,2048]{2,1,0:T(8,128)(2,1)} %bitcast.49), calls=%async_computation.3 | async-start | bytes 4194304 | tf_op jit(solution)/shard_map/all_to_all | solution.py:277
  220.0 4.6 %copy-start.14 = (bf16[2048,1024]{1,0:T(8,128)(2,1)S(1)}, bf16[2048,1024]{1,0:T(8,128)(2,1)}, u32[]{:S(2)}) copy-start(bf16[2048,1024]{1,0:T(8,128)(2,1)} %param.19) | copy-start | bytes 12582916
  232.2 4.9 %copy-start.2 = (bf16[1536,1024]{1,0:T(8,128)(2,1)}, bf16[1536,1024]{1,0:T(8,128)(2,1)S(1)}, u32[]{:S(2)}) copy-start(bf16[1536,1024]{1,0:T(8,128)(2,1)S(1)} %fusion.44) | copy-start | bytes 9437188
  237.1 19.2 %collective-permute-start.11 = (bf16[128,1024]{1,0:T(8,128)(2,1)}, bf16[128,1024]{1,0:T(8,128)(2,1)S(1)}, u32[]{:S(2)}, u32[]{:S(2)}) collective-permute-start(bf16[128,1024]{1,0:T(8,128)(2,1)} %get-tuple-element.15), channel_id=1, source_target_pairs={{0,1},{1,0},{2,3},{3,2},{4,7},{5,6},{6,5},{7,4},{8,9},{9,8},{10,11... | collective-permute-start | bytes 786440 | tf_op jit(solution)/shard_map/ppermute | solution.py:52
  237.1 22.5 %collective-permute-start.12 = (bf16[128,1024]{1,0:T(8,128)(2,1)}, bf16[128,1024]{1,0:T(8,128)(2,1)S(1)}, u32[]{:S(2)}, u32[]{:S(2)}) collective-permute-start(bf16[128,1024]{1,0:T(8,128)(2,1)} %get-tuple-element.16), channel_id=1, source_target_pairs={{0,4},{1,5},{2,6},{3,7},{4,0},{5,1},{6,2},{7,3},{8,12},{9,13},{10,... | collective-permute-start | bytes 786440 | tf_op jit(solution)/shard_map/ppermute | solution.py:52
  238.9 17.5 %copy-start.4 = (f32[128,1024]{1,0:T(8,128)S(1)}, f32[128,1024]{1,0:T(8,128)}, u32[]{:S(2)}) copy-start(f32[128,1024]{1,0:T(8,128)} %get-tuple-element.14) | copy-start | bytes 1572868
  238.9 20.8 %collective-permute-start.13 = (bf16[128,1024]{1,0:T(8,128)(2,1)}, bf16[128,1024]{1,0:T(8,128)(2,1)S(1)}, u32[]{:S(2)}, u32[]{:S(2)}) collective-permute-start(bf16[128,1024]{1,0:T(8,128)(2,1)} %get-tuple-element.17), channel_id=1, source_target_pairs={{0,5},{1,4},{2,7},{3,6},{4,3},{5,2},{6,1},{7,0},{8,13},{9,12},{10,... | collective-permute-start | bytes 786440 | tf_op jit(solution)/shard_map/ppermute | solution.py:52
  253.0 6.8 %copy-start.5 = (f32[128,1024]{1,0:T(8,128)S(1)}, f32[128,1024]{1,0:T(8,128)}, u32[]{:S(2)}) copy-start(f32[128,1024]{1,0:T(8,128)} %get-tuple-element.18) | copy-start | bytes 1572868
  253.0 6.6 %collective-permute-start.15 = (bf16[128,1024]{1,0:T(8,128)(2,1)}, bf16[128,1024]{1,0:T(8,128)(2,1)S(1)}, u32[]{:S(2)}, u32[]{:S(2)}) collective-permute-start(bf16[128,1024]{1,0:T(8,128)(2,1)} %get-tuple-element.19), channel_id=1, source_target_pairs={{0,1},{1,0},{2,3},{3,2},{4,7},{5,6},{6,5},{7,4},{8,9},{9,8},{10,11... | collective-permute-start | bytes 786440 | tf_op jit(solution)/shard_map/ppermute | solution.py:52
  253.0 6.9 %collective-permute-start.16 = (bf16[128,1024]{1,0:T(8,128)(2,1)}, bf16[128,1024]{1,0:T(8,128)(2,1)S(1)}, u32[]{:S(2)}, u32[]{:S(2)}) collective-permute-start(bf16[128,1024]{1,0:T(8,128)(2,1)} %get-tuple-element.20), channel_id=1, source_target_pairs={{0,4},{1,5},{2,6},{3,7},{4,0},{5,1},{6,2},{7,3},{8,12},{9,13},{10,... | collective-permute-start | bytes 786440 | tf_op jit(solution)/shard_map/ppermute | solution.py:52
  256.3 8.7 %collective-permute-start.17 = (bf16[128,1024]{1,0:T(8,128)(2,1)}, bf16[128,1024]{1,0:T(8,128)(2,1)S(1)}, u32[]{:S(2)}, u32[]{:S(2)}) collective-permute-start(bf16[128,1024]{1,0:T(8,128)(2,1)} %get-tuple-element.21), channel_id=1, source_target_pairs={{0,5},{1,4},{2,7},{3,6},{4,3},{5,2},{6,1},{7,0},{8,13},{9,12},{10,... | collective-permute-start | bytes 786440 | tf_op jit(solution)/shard_map/ppermute | solution.py:52

commit v2 on v1

v2 whole, which is shorter than its diff:
```python
import jax
import jax.numpy as jnp
from jax import lax
from jax.experimental import pallas as pl
from jax.experimental.pallas import tpu as pltpu
from jax.sharding import Mesh
from jax.sharding import PartitionSpec as P

EXPERTS = 32
TOP = 2
MOE_DEV = 128
CAP = 16
PLANES = 16
CHUNKS = 2
EP_TP = ("ep_0", "ep_1", "ep_2", "tp")
EP = ("ep_0", "ep_1", "ep_2")
CHIPS = ("ep_0", "ep_1")
CORE_TP = ("ep_2", "tp")

epsilon = 1e-06
f32 = jnp.float32
bf16 = jnp.bfloat16


def ring_pairs(move):
    pairs = []
    for core in range(2):
        for x in range(4):
            to_core, to_x = move(core, x)
            pairs.append((core * 4 + x, to_core * 4 + to_x))
    return pairs


def weight_partner(core, x):
    return core, (((x - core) % 4 ^ 1) + core) % 4


def hidden_partner(core, x):
    return core, ((3 - (x - core) % 4) + core) % 4


def other_core(core, x):
    return 1 - core, x


def diagonal(core, x):
    return 1 - core, weight_partner(core, x)[1]


def swapped(value, move):
    return lax.ppermute(value, CORE_TP, ring_pairs(move))


def exchanged(blocks):
    return lax.all_to_all(blocks, CHIPS, split_axis=0, concat_axis=0, tiled=True)


def params(mib):
    return pltpu.CompilerParams(vmem_limit_bytes=mib << 20)


def cost(microseconds, mib):
    return pl.CostEstimate(
        flops=int(microseconds * 7e8), bytes_accessed=mib << 20, transcendentals=0
    )


def block_slots(info, core):
    picks = info[0:TOP, :].astype(jnp.int32)
    first, second = picks[0:1, :], picks[1:2, :]
    count = info.shape[1]
    experts = lax.broadcasted_iota(jnp.int32, (EXPERTS, count), 0)
    in_first, in_second = first == experts, second == experts
    named = jnp.where(in_first | in_second, 1.0, 0.0).astype(bf16)
    earlier = (
        lax.broadcasted_iota(jnp.int32, (count, count), 0)
        < lax.broadcasted_iota(jnp.int32, (count, count), 1)
    )
    before = jnp.dot(
        named, jnp.where(earlier, 1.0, 0.0).astype(bf16), preferred_element_type=f32
    )
    slots = []
    for pick, mask in ((first, in_first), (second, in_second)):
        position = jnp.sum(jnp.where(mask, before, 0.0), axis=0, keepdims=True)
        slot = (pick >> 1) * CAP + position.astype(jnp.int32)
        slots.append(jnp.where((pick & 1) == core, slot, -1))
    return slots


def dispatch_kernel(where, x_ref, info_ref, gain_ref, out_ref):
    width = 1024
    widened = x_ref[...].astype(f32)
    inverse = lax.rsqrt(jnp.mean(widened * widened, axis=-1, keepdims=True) + epsilon)
    slot_a, slot_b = block_slots(info_ref[...], where[1])
    slots = lax.broadcasted_iota(jnp.int32, (PLANES * CAP, MOE_DEV), 0)
    spread = jnp.where((slots == slot_a) | (slots == slot_b), 1.0, 0.0).astype(bf16)

    depth = out_ref.shape[2]
    first = 0 if depth == x_ref.shape[1] else where[7] * depth

    def piece(k, carry):
        cols = pl.ds(pl.multiple_of(first + k * width, width), width)
        normed = (x_ref[:, cols].astype(f32) * inverse * gain_ref[:, cols]).astype(bf16)
        rows = jnp.dot(spread, normed, preferred_element_type=f32).astype(bf16)
        out_ref[:, :, pl.ds(pl.multiple_of(k * width, width), width)] = rows.reshape(
            PLANES, CAP, width
        )
        return carry

    lax.fori_loop(0, depth // width, piece, 0)


def dispatch(where, rows, info, gain, whole_rows, out_depth):
    depth = rows.shape[1]
    row_block = lambda i, w: (w[0] * 2 + i, 0)
    return pl.pallas_call(
        dispatch_kernel,
        grid_spec=pltpu.PrefetchScalarGridSpec(
            num_scalar_prefetch=1,
            grid=(2,),
            in_specs=[
                pl.BlockSpec((MOE_DEV, depth), row_block if whole_rows else lambda i, w: (i, 0)),
                pl.BlockSpec((info.shape[0], MOE_DEV), lambda i, w: (0, w[0] * 2 + i)),
                pl.BlockSpec((1, depth), lambda i, w: (0, 0)),
            ],
            out_specs=pl.BlockSpec((PLANES, CAP, out_depth), lambda i, w: (0, i, 0)),
        ),
        out_shape=jax.ShapeDtypeStruct((PLANES, 2 * CAP, out_depth), bf16),
        cost_estimate=cost(6, 6),
        name="dispatch",
    )(where, rows, info, gain)


def hidden_kernel(where, low, high, gate_own, up_own, gate_part, up_part, out_ref, totals):
    step, steps = pl.program_id(0), pl.num_programs(0)
    width = gate_own.shape[1]

    @pl.when(step == 0)
    def _():
        totals[...] = jnp.zeros_like(totals)

    def add(block):
        for i, ref in enumerate((gate_own, up_own, gate_part, up_part)):
            totals[i] += jnp.dot(block, ref[...], preferred_element_type=f32)

    @pl.when(step < steps // 2)
    def _():
        add(low[...])

    @pl.when(step >= steps // 2)
    def _():
        add(high[...])

    @pl.when(step == steps - 1)
    def _():
        for i in range(2):
            value = jax.nn.silu(totals[2 * i]) * totals[2 * i + 1]
            out_ref[:, i * width : (i + 1) * width] = value.astype(bf16)


def hidden_units(where, low, high, gate_own, up_own, gate_part, up_part):
    depth, width = gate_own.shape
    rows = low.shape[0]
    step = 1024
    half = depth // step // 2
    if low is high:
        order = lambda k, w: k
        high_block = lambda k, w: (0, jnp.maximum(k, half))
    else:
        order = lambda k, w: lax.rem(k + w[7] * half, 2 * half)
        high_block = lambda k, w: (0, jnp.maximum(k - half, 0))
    weight = pl.BlockSpec((step, width), lambda k, w: (order(k, w), 0))
    return pl.pallas_call(
        hidden_kernel,
        grid_spec=pltpu.PrefetchScalarGridSpec(
            num_scalar_prefetch=1,
            grid=(2 * half,),
            in_specs=[
                pl.BlockSpec((rows, step), lambda k, w: (0, jnp.minimum(k, half - 1))),
                pl.BlockSpec((rows, step), high_block),
            ]
            + [weight] * 4,
            out_specs=pl.BlockSpec((rows, 2 * width), lambda k, w: (0, 0)),
            scratch_shapes=[pltpu.VMEM((4, rows, width), f32)],
        ),
        out_shape=jax.ShapeDtypeStruct((rows, 2 * width), bf16),
        cost_estimate=cost(10, 12),
        name="hidden",
    )(where, low, high, gate_own, up_own, gate_part, up_part)


def down_kernel(where, near, far, own_ref, part_ref, out_ref):
    quarter = near.shape[1] // 2

    def run(weight):
        total = None
        for i in range(4):
            source = (near, far)[i // 2]
            values = source[:, (i % 2) * quarter : (i % 2 + 1) * quarter]
            rows = pl.ds(pl.multiple_of(where[2 + i] * quarter, quarter), quarter)
            product = jnp.dot(values, weight[rows, :], preferred_element_type=f32)
            total = product if total is None else total + product
        out_ref[...] = total.astype(bf16).reshape(out_ref.shape)

    @pl.when(pl.program_id(0) < 2)
    def _():
        run(own_ref)

    @pl.when(pl.program_id(0) >= 2)
    def _():
        run(part_ref)


def down_result(where, near, far, down_own, down_part):
    rows = near.shape[0]
    depth, width = down_own.shape
    step = width // 2
    whole = pl.BlockSpec(near.shape, lambda j, w: (0, 0))
    return pl.pallas_call(
        down_kernel,
        grid_spec=pltpu.PrefetchScalarGridSpec(
            num_scalar_prefetch=1,
            grid=(4,),
            in_specs=[
                whole,
                whole,
                pl.BlockSpec((depth, step), lambda j, w: (0, jnp.minimum(j, 1))),
                pl.BlockSpec((depth, step), lambda j, w: (0, jnp.maximum(j - 2, 0))),
            ],
            out_specs=pl.BlockSpec((PLANES, rows // PLANES, step), lambda j, w: (0, 0, j)),
        ),
        out_shape=jax.ShapeDtypeStruct((PLANES, rows // PLANES, 2 * width), bf16),
        cost_estimate=cost(5, 7),
        name="down",
    )(where, near, far, down_own, down_part)


def combine_kernel(where, info_ref, result_ref, own_slice, other_slice):
    half = own_slice.shape[1]
    info = info_ref[...]
    slot_a, slot_b = block_slots(info, where[1])
    slots = lax.broadcasted_iota(jnp.int32, (PLANES * CAP, MOE_DEV), 0)
    weights = jnp.where(slots == slot_a, info[2:3, :], 0.0) + jnp.where(
        slots == slot_b, info[3:4, :], 0.0
    )
    coarse = weights.astype(bf16)
    fine = weights - coarse.astype(f32)
    table = jnp.concatenate([coarse.astype(f32).T, fine.T], axis=0).astype(bf16)
    for part, ref in enumerate((own_slice, other_slice)):
        rows = result_ref[:, :, part * half : (part + 1) * half].reshape(PLANES * CAP, half)
        total = jnp.dot(table, rows, preferred_element_type=f32)
        ref[...] = (total[:MOE_DEV] + total[MOE_DEV:]).astype(ref.dtype)


def combine(where, info, returned, own_type):
    half = returned.shape[2] // 2
    out = pl.BlockSpec((MOE_DEV, half), lambda i, w: (i, 0))
    return pl.pallas_call(
        combine_kernel,
        grid_spec=pltpu.PrefetchScalarGridSpec(
            num_scalar_prefetch=1,
            grid=(2,),
            in_specs=[
                pl.BlockSpec((4, MOE_DEV), lambda i, w: (0, w[0] * 2 + i)),
                pl.BlockSpec((PLANES, CAP, 2 * half), lambda i, w: (0, i, 0)),
            ],
            out_specs=[out, out],
        ),
        out_shape=[jax.ShapeDtypeStruct((2 * MOE_DEV, half), t) for t in (own_type, bf16)],
        cost_estimate=cost(4, 4),
        compiler_params=params(12),
        name="combine",
    )(where, info, returned)


def total_kernel(where, keep, partner, sib, diag, out_ref):
    half = pl.program_id(0)

    def add(mine, theirs):
        out_ref[...] = (mine[...].astype(f32) + theirs[...].astype(f32)).astype(bf16)

    for own_place in range(2):
        for sib_place in range(2):

            @pl.when(((half == where[0]) == (own_place == 0)) & ((half == where[6]) == (sib_place == 0)))
            def _():
                add((keep, partner)[own_place], (sib, diag)[sib_place])


def total_rows(where, keep, partner, sib, diag):
    rows, width = keep.shape
    whole = pl.BlockSpec((rows, width), lambda i, w: (0, 0))
    return pl.pallas_call(
        total_kernel,
        grid_spec=pltpu.PrefetchScalarGridSpec(
            num_scalar_prefetch=1,
            grid=(2,),
            in_specs=[whole] * 4,
            out_specs=pl.BlockSpec((rows, width), lambda i, w: (i, 0)),
        ),
        out_shape=jax.ShapeDtypeStruct((2 * rows, width), bf16),
        cost_estimate=cost(3, 4),
        compiler_params=params(12),
        name="total",
    )(where, keep, partner, sib, diag)


def gated_rows(value, gate):
    return (value.astype(f32) * jax.nn.sigmoid(gate.astype(f32))).astype(bf16)


def conv_kernel(
    value_ref, gate_ref, halo_ref, taps_ref, gain_ref, bias_ref, top_ref, bottom_ref, rows, mixed
):
    reach = halo_ref.shape[0]
    block = value_ref.shape[0]
    lanes = 128

    @pl.when(pl.program_id(0) == 0)
    def _():
        rows[:reach, :] = halo_ref[...].astype(f32)

    @pl.when(pl.program_id(0) > 0)
    def _():
        rows[:reach, :] = rows[block:, :]

    rows[reach:, :] = gated_rows(value_ref[...], gate_ref[...]).astype(f32)

    def piece(k, carry):
        cols = pl.ds(pl.multiple_of(k * lanes, lanes), lanes)
        column = rows[:, cols]
        total = jnp.zeros((block, lanes), f32)
        for phase in range(8):
            moved = column if phase == 0 else pltpu.roll(column, phase, 0)
            for lag in range(phase, taps_ref.shape[0], 8):
                start = reach - (lag - phase)
                total = total + taps_ref[lag : lag + 1, cols] * moved[start : start + block]
        mixed[:, cols] = total
        return carry

    lax.fori_loop(0, mixed.shape[1] // lanes, piece, 0)
    whole = mixed[...]
    center = whole - jnp.mean(whole, axis=-1, keepdims=True)
    spread = jnp.mean(center * center, axis=-1, keepdims=True)
    scaled = center * lax.rsqrt(spread + epsilon) * gain_ref[...] + bias_ref[...]
    result = jax.nn.silu(scaled).astype(bf16)
    half = pl.num_programs(0) // 2

    @pl.when(pl.program_id(0) < half)
    def _():
        top_ref[...] = result

    @pl.when(pl.program_id(0) >= half)
    def _():
        bottom_ref[...] = result


def conv_rows(conv_value, conv_gate, earlier, conv_taps, conv_gain, conv_bias):
    length, width = conv_value.shape
    block = 64
    half = length // block // 2
    reach = earlier.shape[0]
    row_block = pl.BlockSpec((block, width), lambda i: (i, 0))
    whole = lambda rows: pl.BlockSpec((rows, width), lambda i: (0, 0))
    return pl.pallas_call(
        conv_kernel,
        grid=(length // block,),
        in_specs=[row_block, row_block, whole(reach), whole(conv_taps.shape[0]), whole(1), whole(1)],
        out_specs=[
            pl.BlockSpec((block, width), lambda i: (jnp.minimum(i, half - 1), 0)),
            pl.BlockSpec((block, width), lambda i: (jnp.maximum(i - half, 0), 0)),
        ],
        out_shape=[jax.ShapeDtypeStruct((length // 2, width), bf16)] * 2,
        scratch_shapes=[
            pltpu.VMEM((reach + block, width), f32),
            pltpu.VMEM((block, width), f32),
        ],
        cost_estimate=cost(14, 5),
        compiler_params=params(12),
    )(conv_value, conv_gate, earlier, conv_taps, conv_gain[None], conv_bias[None])


def work(
    conv_value,
    conv_gate,
    conv_taps,
    conv_gain,
    conv_bias,
    conv_projection,
    expert_input,
    expert_gain,
    route_experts,
    group_gate,
    expert_gate,
    gate_weight,
    up_weight,
    down_weight,
):
    core, x = lax.axis_index("ep_2"), lax.axis_index("tp")
    place = (x - core) % 4

    def half_of(which_core):
        spot = (x - which_core) % 4
        return ((spot == 1) | (spot == 2)).astype(jnp.int32)

    half, sib_half = half_of(core), half_of(1 - core)
    hidden_order = [place, place ^ 1, 3 - place, (3 - place) ^ 1]
    quarters = [(p + core) % 4 for p in hidden_order]
    where = jnp.stack([half, core, *quarters, sib_half, place >> 1]).astype(jnp.int32)
    rows_half = expert_input.shape[0] // 2
    gate_own, up_own, down_own = gate_weight[0], up_weight[0], down_weight[0]
    gain = expert_gain[None]

    outgoing = lax.dynamic_slice_in_dim(expert_input, sib_half * rows_half, rows_half, 0)
    sib_rows = swapped(outgoing, other_core)
    share = group_gate[:, None] * expert_gate / jnp.sum(expert_gate, axis=1, keepdims=True)
    info = jnp.concatenate([route_experts.astype(f32).T, share.T], axis=0)
    sib_info = swapped(info, other_core)
    gate_part = swapped(gate_own, weight_partner)
    up_part = swapped(up_own, weight_partner)

    infos = (info, sib_info)
    depth = expert_input.shape[1]
    first = dispatch(where, expert_input, route_experts.T, gain, True, depth // 2)
    first_arrived = exchanged(first)
    second = dispatch(where, sib_rows, sib_info, gain, False, depth)
    second, first_arrived = lax.optimization_barrier((second, first_arrived))
    second_arrived = exchanged(second).reshape(-1, depth)
    low = first_arrived.reshape(-1, depth // 2)
    high = swapped(low, hidden_partner)
    arrived = ((low, high), (second_arrived, second_arrived))

    reach = 32
    tail = gated_rows(conv_value[-reach:], conv_gate[-reach:])
    count = lax.axis_size(EP_TP)
    earlier = lax.ppermute(tail, EP_TP, [(k, k + 1) for k in range(count - 1)])
    conv_value, conv_gate, _ = lax.optimization_barrier((conv_value, conv_gate, first))
    top, bottom = conv_rows(
        conv_value, conv_gate, earlier, conv_taps, conv_gain, conv_bias
    )
    down_part = swapped(down_own, weight_partner)

    combined = []
    for k in range(CHUNKS):
        near = hidden_units(where, *arrived[k], gate_own, up_own, gate_part, up_part)
        far = swapped(near, hidden_partner)
        result = down_result(where, near, far, down_own, down_part)
        returned = exchanged(result)
        combined.append(combine(where, infos[k], returned, (f32, bf16)[k]))
    keep, from_partner = combined[0][0], swapped(combined[0][1], weight_partner)
    from_sib = swapped(combined[1][0], other_core)
    from_diag = swapped(combined[1][1], diagonal)
    expert_out = total_rows(where, keep, from_partner, from_sib, from_diag)

    rows = conv_value.shape[0]
    middle = rows // 2
    right = [(k, (k + 1) % 4) for k in range(4)]
    left = [(k, (k - 1) % 4) for k in range(4)]

    def passed(value, pairs):
        return lax.ppermute(value, "tp", pairs)

    left_top = passed(top, right)
    right_bottom = passed(bottom, left)
    left_bottom = passed(bottom, right)
    right_top = passed(top, left)
    far_top = passed(left_top, right)
    far_bottom = passed(right_bottom, left)
    conv_out = jnp.zeros((4 * rows, conv_projection.shape[1]), bf16)
    for block, offset, start in (
        (top, 0, 0),
        (bottom, 0, middle),
        (left_top, 3, 0),
        (right_bottom, 1, middle),
        (left_bottom, 3, middle),
        (right_top, 1, 0),
        (far_top, 2, 0),
        (far_bottom, 2, middle),
    ):
        product = jnp.dot(block, conv_projection, preferred_element_type=f32).astype(bf16)
        conv_out = lax.dynamic_update_slice_in_dim(
            conv_out, product, (x + offset) % 4 * rows + start, 0
        )
    return (conv_out, expert_out)


def solution(mesh):
    finer = Mesh(mesh.devices.reshape(4, 4, 2, mesh.shape["tp"]), EP_TP)
    in_specs = (
        P(EP_TP, None),
        P(EP_TP, None),
        P(),
        P(),
        P(),
        P(None, "tp"),
        P(EP, None),
        P(),
        P(EP, None),
        P(EP),
        P(EP, None),
        P(EP, None, "tp"),
        P(EP, None, "tp"),
        P(EP, None, "tp"),
    )
    out_specs = (P(EP, "tp"), P(EP, "tp"))
    return jax.shard_map(work, mesh=finer, in_specs=in_specs, out_specs=out_specs, check_vma=False)
```

time: 272 us -> 271 us (level); the launches traced: 267 us -> 270 us
  other arithmetic: 55.4 us -> 1.09 us
  Pallas kernels: 21.6 us -> 66.2 us
  waiting for transfers between devices: 74.7 us -> 118 us
  matrix products: 55.2 us -> 22.9 us
  starting transfers between devices: 44.9 us -> 49 us
    ppermute x13 -> x11, waiting for transfers between devices: 27.7 us -> 83 us  [swapped(): return lax.ppermute(value, CORE_TP, ring_pairs(move))]
    pallas_call x0 -> x6, Pallas kernels: none -> 49.6 us  [the longest x2 19.6 us: hidden_units(): pl.pallas_call(hidden_kernel, grid_spec=pltpu.PrefetchScalarGridSpec(num_...]
    concatenate x4 -> x1, other arithmetic: 34.1 us -> 0.01 us  [work(): info = jnp.concatenate([route_experts.astype(f32).T, share.T], axis=0)]
    dot_general x17 -> x8, matrix products: 55.2 us -> 22.9 us  [work(): jnp.dot(block, conv_projection, preferred_element_type=f32).astype(bf16)]
    all_to_all x4, waiting for transfers between devices: 46.9 us -> 24.6 us  [exchanged(): lax.all_to_all(blocks, CHIPS, split_axis=0, concat_axis=0, tiled=True)]
    reduce_sum x3 -> x1, other arithmetic: 14.9 us -> 0.02 us  [work(): jnp.sum(expert_gate, axis=1, keepdims=True)]
    ppermute x5 -> x7, waiting for transfers between devices: 0.01 us -> 10.4 us  [the longest x6 10.4 us: passed(): return lax.ppermute(value, 'tp', pairs)]
    unnamed x38 -> x42, local copies, waits for them, and re-layouts: 2.43 us -> 9.53 us
  transfers between devices with their start and end apart: 22 -> 22, of which waited for: 7 -> 7; matrix products, arithmetic and copies ran while one was open for 44% -> 9% of each run, Pallas kernels for 6% -> 24%
where the time goes in v2:
time: 271 us; the launch traced here: 270 us
  waiting for transfers between devices  118 us (44%)
  Pallas kernels  66.2 us (24%)
  starting transfers between devices  49 us (18%)
  matrix products  22.9 us (8%)
  local copies, waits for them, and re-layouts  12.3 us (5%)
    ppermute x11, waiting for transfers between devices, swapped(): return lax.ppermute(value, CORE_TP, ring_pairs(move))  83 us
    all_to_all x4, starting transfers between devices, exchanged(): lax.all_to_all(blocks, CHIPS, split_axis=0, concat_axis=0, tiled=True)  25.8 us
    all_to_all x4, waiting for transfers between devices, exchanged(): lax.all_to_all(blocks, CHIPS, split_axis=0, concat_axis=0, tiled=True)  24.6 us
    dot_general x8, matrix products, work(): jnp.dot(block, conv_projection, preferred_element_type=f32).astype(bf16)  22.9 us
    pallas_call x2, Pallas kernels, hidden_units(): pl.pallas_call(hidden_kernel, grid_spec=pltpu.PrefetchScalarGridSpec(num_...  19.6 us
    pallas_call x1, Pallas kernels, conv_rows(): pl.pallas_call(conv_kernel, grid=(length // block,), in_specs=[row_block,...  14.4 us
    pallas_call x2, Pallas kernels, down_result(): pl.pallas_call(down_kernel, grid_spec=pltpu.PrefetchScalarGridSpec(num_sc...  14 us
    ppermute x11, starting transfers between devices, swapped(): return lax.ppermute(value, CORE_TP, ring_pairs(move))  12.5 us
  transfers between devices with their start and end apart: 22, of which 7 were waited for; matrix products, arithmetic and copies ran while one was open for 9% of the time, Pallas kernels for 24%

profile of v2, /device:TPU:1, one launch (start us, length us, event | category | flops | bytes accessed | tf_op | source)
XLA Modules:
  0.0 270.4 jit_solution(3680807912802490541)
XLA Ops:
  0.7 1.7 constant_dynamic-slice_fusion
  2.4 1.5 collective-permute-start.7
  3.9 0.7 stack.43.where
  4.5 4.8 %dispatch.2 = bf16[16,32,2048]{2,1,0:T(8,128)(2,1)} custom-call(s32[8]{0:T(128)} %stack.43.where, bf16[512,4096]{1,0:T(8,128)(2,1)} %x_ref.1, s32[2,512]{1,0:T(2,128)} %bitcast.39, f32[1,4096]{1,0:T(1,128)} %bitcast.49), custom_call_target="tpu_custom_call" | custom-call | flops 4200000000 | bytes 6291456 | tf_op jit(solution)/shard_map/dispatch/pallas_call | solution.py:116
  9.3 8.1 %all-to-all-start = ((bf16[16,32,2048]{2,1,0:T(8,128)(2,1)}), bf16[16,32,2048]{2,1,0:T(8,128)(2,1)}, u32[]{:S(2)}, u32[]{:S(2)}) async-start(bf16[16,32,2048]{2,1,0:T(8,128)(2,1)} %dispatch.2), calls=%async_computation | async-start | bytes 4194304 | tf_op jit(solution)/shard_map/all_to_all | solution.py:55
  17.5 0.5 collective-permute-start.8
  18.0 0.8 collective-permute-done.8.info_ref
  18.8 0.0 collective-permute-done.7.x_ref
  18.8 0.6 copy-done.6
  19.4 6.4 %dispatch.3 = bf16[16,32,4096]{2,1,0:T(8,128)(2,1)} custom-call(s32[8]{0:T(128)} %stack.43.where, bf16[256,4096]{1,0:T(8,128)(2,1)} %collective-permute-done.7.x_ref, f32[4,512]{1,0:T(4,128)} %copy-done.6, f32[1,4096]{1,0:T(1,128)} %bitcast.50), custom_call_target="tpu_custom_call" | custom-call | flops 4200000000 | bytes 6291456 | tf_op jit(solution)/shard_map/dispatch/pallas_call | solution.py:116
  25.8 24.6 %all-to-all-done = bf16[16,32,2048]{2,1,0:T(8,128)(2,1)} async-done(((bf16[16,32,2048]{2,1,0:T(8,128)(2,1)}), bf16[16,32,2048]{2,1,0:T(8,128)(2,1)}, u32[]{:S(2)}, u32[]{:S(2)}) %all-to-all-start) | async-done | bytes 2097184 | tf_op jit(solution)/shard_map/all_to_all | solution.py:55
  50.5 4.6 %all-to-all-start.2 = ((bf16[16,32,4096]{2,1,0:T(8,128)(2,1)}), bf16[16,32,4096]{2,1,0:T(8,128)(2,1)}, u32[]{:S(2)}, u32[]{:S(2)}) async-start(bf16[16,32,4096]{2,1,0:T(8,128)(2,1)} %dispatch.3), calls=%async_computation.2 | async-start | bytes 8388608 | tf_op jit(solution)/shard_map/all_to_all | solution.py:55
  55.0 2.5 collective-permute-start.10
  57.6 0.2 collective-permute-start.11
  57.8 2.5 collective-permute-start.13
  60.2 39.9 %collective-permute-done.10.gate_part = bf16[4096,256]{1,0:T(8,128)(2,1)S(1)} collective-permute-done((bf16[4096,256]{1,0:T(8,128)(2,1)S(1)}, bf16[4096,256]{1,0:T(8,128)(2,1)S(1)}, u32[]{:S(2)}, u32[]{:S(2)}) %collective-permute-start.10) | collective-permute-done | bytes 2097184 | tf_op jit(solution)/shard_map/ppermute | solution.py:51
  100.1 1.3 copy-done.18
  101.4 24.7 %collective-permute-done.11.up_part = bf16[4096,256]{1,0:T(8,128)(2,1)S(1)} collective-permute-done((bf16[4096,256]{1,0:T(8,128)(2,1)}, bf16[4096,256]{1,0:T(8,128)(2,1)S(1)}, u32[]{:S(2)}, u32[]{:S(2)}) %collective-permute-start.11) | collective-permute-done | bytes 2097184 | tf_op jit(solution)/shard_map/ppermute | solution.py:51
  126.1 1.3 copy-done.19
  127.4 9.7 %hidden.2.near = bf16[512,512]{1,0:T(8,128)(2,1)} custom-call(s32[8]{0:T(128)} %stack.43.where, bf16[512,2048]{1,0:T(8,128)(2,1)} %bitcast.14.low, bf16[512,2048]{1,0:T(8,128)(2,1)} %collective-permute-done.9.high, bf16[4096,256]{1,0:T(8,128)(2,1)} %bitcast.40, bf16[4096,256]{1,0:T(8,128)(2,1)} %bitcast.44, bf16[4096,256]{1,0:T(8,128)(2,1)} %copy-done.18, ...), custom_call_target="tpu_custom_call" | custom-call | flops 7000000000 | bytes 12582912 | tf_op jit(solution)/shard_map/hidden/pallas_call | solution.py:173
  137.1 0.3 collective-permute-start.12
  137.4 1.0 multiply_convert_fusion
  138.5 3.1 %collective-permute-start = (bf16[32,2048]{1,0:T(8,128)(2,1)S(1)}, bf16[32,2048]{1,0:T(8,128)(2,1)S(1)}, u32[]{:S(2)}, u32[]{:S(2)}) collective-permute-start(bf16[32,2048]{1,0:T(8,128)(2,1)S(1)} %multiply_convert_fusion), channel_id=1, source_target_pairs={{0,1},{1,2},{2,3},{3,4},{4,5},{5,6},{6,7},{7,8},{8,9},{9,10},{10,1... | collective-permute-start | bytes 393224 | tf_op jit(solution)/shard_map/ppermute | solution.py:436
  141.7 13.1 %collective-permute-done.13.part_ref = bf16[1024,1024]{1,0:T(8,128)(2,1)} collective-permute-done((bf16[1024,1024]{1,0:T(8,128)(2,1)}, bf16[1024,1024]{1,0:T(8,128)(2,1)}, u32[]{:S(2)}, u32[]{:S(2)}) %collective-permute-start.13) | collective-permute-done | bytes 2097184 | tf_op jit(solution)/shard_map/ppermute | solution.py:51
  154.7 0.8 copy-done.20
  155.5 7.0 %down.2 = bf16[16,32,2048]{2,1,0:T(8,128)(2,1)} custom-call(s32[8]{0:T(128)} %stack.43.where, bf16[512,512]{1,0:T(8,128)(2,1)} %hidden.2.near, bf16[512,512]{1,0:T(8,128)(2,1)} %copy-done.20, bf16[1024,1024]{1,0:T(8,128)(2,1)} %bitcast.47, bf16[1024,1024]{1,0:T(8,128)(2,1)} %collective-permute-done.13.part_ref), custom_call_target="tpu_custom_call" | custom-call | flops 3500000000 | bytes 7340032 | tf_op jit(solution)/shard_map/down/pallas_call | solution.py:219
  162.6 6.4 %all-to-all-start.1 = ((bf16[16,32,2048]{2,1,0:T(8,128)(2,1)}), bf16[16,32,2048]{2,1,0:T(8,128)(2,1)S(1)}, u32[]{:S(2)}, u32[]{:S(2)}) async-start(bf16[16,32,2048]{2,1,0:T(8,128)(2,1)} %down.2), calls=%async_computation.1 | async-start | bytes 4194304 | tf_op jit(solution)/shard_map/all_to_all | solution.py:55
  169.0 0.0 copy-start.3
  169.0 0.0 copy-start.4
  169.0 0.0 copy-start.5
  169.0 9.9 %hidden.3.near = bf16[512,512]{1,0:T(8,128)(2,1)} custom-call(s32[8]{0:T(128)} %stack.43.where, bf16[512,4096]{1,0:T(8,128)(2,1)} %bitcast.18.low.high, bf16[512,4096]{1,0:T(8,128)(2,1)} %bitcast.18.low.high, bf16[4096,256]{1,0:T(8,128)(2,1)} %bitcast.41, bf16[4096,256]{1,0:T(8,128)(2,1)} %bitcast.45, bf16[4096,256]{1,0:T(8,128)(2,1)} %copy-done.18, ...), custom_call_target="tpu_custom_call" | custom-call | flops 7000000000 | bytes 12582912 | tf_op jit(solution)/shard_map/hidden/pallas_call | solution.py:173
  178.9 0.0 collective-permute-start.15
  178.9 0.0 copy-start
  178.9 1.4 copy-done
  180.3 1.4 copy-done.1
  181.8 14.4 %shard_map.149 = (bf16[192,2048]{1,0:T(8,128)(2,1)S(1)}, bf16[192,2048]{1,0:T(8,128)(2,1)}) custom-call(bf16[384,2048]{1,0:T(8,128)(2,1)S(1)} %copy-done, bf16[384,2048]{1,0:T(8,128)(2,1)S(1)} %copy-done.1, bf16[32,2048]{1,0:T(8,128)(2,1)S(1)} %collective-permute-done.halo_ref, f32[31,2048]{1,0:T(8,128)S(1)} %copy-done.3, f32[1,2048]{1,0:T(1,128)S(1)} %bitcast.37, ...), custom_call_target="tpu_custom_call" | custom-call | flops 9799999488 | bytes 5242880 | tf_op jit(solution)/shard_map/pallas_call | solution.py:365
  196.2 2.3 collective-permute-start.2
  198.5 0.8 collective-permute-start.1
  199.3 1.9 collective-permute-start.4
  201.2 0.4 broadcast_in_dim.14
  201.6 1.0 fusion.7
  202.6 0.0 copy-start.10
  202.6 1.7 copy-done.10
  204.2 6.9 %down.3 = bf16[16,32,2048]{2,1,0:T(8,128)(2,1)} custom-call(s32[8]{0:T(128)} %stack.43.where, bf16[512,512]{1,0:T(8,128)(2,1)} %hidden.3.near, bf16[512,512]{1,0:T(8,128)(2,1)} %collective-permute-done.15.far, bf16[1024,1024]{1,0:T(8,128)(2,1)} %bitcast.48, bf16[1024,1024]{1,0:T(8,128)(2,1)} %collective-permute-done.13.part_ref), custom_call_target="tpu_custom_call" | custom-call | flops 3500000000 | bytes 7340032 | tf_op jit(solution)/shard_map/down/pallas_call | solution.py:219
  211.2 6.7 %all-to-all-start.3 = ((bf16[16,32,2048]{2,1,0:T(8,128)(2,1)}), bf16[16,32,2048]{2,1,0:T(8,128)(2,1)}, u32[]{:S(2)}, u32[]{:S(2)}) async-start(bf16[16,32,2048]{2,1,0:T(8,128)(2,1)} %down.3), calls=%async_computation.3 | async-start | bytes 4194304 | tf_op jit(solution)/shard_map/all_to_all | solution.py:55
  217.9 0.0 copy-start.15
  217.9 4.3 %fusion.6 = bf16[1536,1024]{1,0:T(8,128)(2,1)} fusion(bf16[1536,1024]{1,0:T(8,128)(2,1)} %copy-done.10, s32[]{:T(128)S(6)} %select_n.86, bf16[192,2048]{1,0:T(8,128)(2,1)} %get-tuple-element.15, bf16[2048,1024]{1,0:T(8,128)(2,1)} %param.19), kind=kOutput, calls=%fused_computation.13 | convolution fusion | flops 805502976 | bytes 5373956 | tf_op jit(solution)/shard_map/dot_general | solution.py:480
  222.2 10.4 %collective-permute-done.1 = bf16[192,2048]{1,0:T(8,128)(2,1)} collective-permute-done((bf16[192,2048]{1,0:T(8,128)(2,1)S(1)}, bf16[192,2048]{1,0:T(8,128)(2,1)}, u32[]{:S(2)}, u32[]{:S(2)}) %collective-permute-start.1) | collective-permute-done | bytes 786464 | tf_op jit(solution)/shard_map/ppermute | solution.py:461
  232.6 2.7 collective-permute-start.6
  235.3 2.9 %fusion.5 = bf16[1536,1024]{1,0:T(8,128)(2,1)} fusion(bf16[1536,1024]{1,0:T(8,128)(2,1)} %fusion.6, s32[]{:T(128)S(6)} %select_n.88, bf16[192,2048]{1,0:T(8,128)(2,1)} %collective-permute-done.1, bf16[2048,1024]{1,0:T(8,128)(2,1)S(1)} %copy-done.15), kind=kOutput, calls=%fused_computation.11 | convolution fusion | flops 805502976 | bytes 5373956 | tf_op jit(solution)/shard_map/dot_general | solution.py:480
  238.2 2.9 %fusion.4 = bf16[1536,1024]{1,0:T(8,128)(2,1)} fusion(bf16[1536,1024]{1,0:T(8,128)(2,1)} %fusion.5, s32[]{:T(128)S(6)} %select_n.90, bf16[192,2048]{1,0:T(8,128)(2,1)} %collective-permute-done.2, bf16[2048,1024]{1,0:T(8,128)(2,1)S(1)} %copy-done.15), kind=kOutput, calls=%fused_computation.9 | convolution fusion | flops 805502976 | bytes 5373956 | tf_op jit(solution)/shard_map/dot_general | solution.py:480
  241.1 2.9 %fusion.3 = bf16[1536,1024]{1,0:T(8,128)(2,1)} fusion(bf16[1536,1024]{1,0:T(8,128)(2,1)} %fusion.4, s32[]{:T(128)S(6)} %select_n.91, bf16[192,2048]{1,0:T(8,128)(2,1)} %collective-permute-done.3, bf16[2048,1024]{1,0:T(8,128)(2,1)S(1)} %copy-done.15), kind=kOutput, calls=%fused_computation.7 | convolution fusion | flops 805502976 | bytes 5373956 | tf_op jit(solution)/shard_map/dot_general | solution.py:480
  244.0 2.9 %fusion.2 = bf16[1536,1024]{1,0:T(8,128)(2,1)} fusion(bf16[1536,1024]{1,0:T(8,128)(2,1)} %fusion.3, s32[]{:T(128)S(6)} %select_n.92, bf16[192,2048]{1,0:T(8,128)(2,1)} %collective-permute-done.4, bf16[2048,1024]{1,0:T(8,128)(2,1)S(1)} %copy-done.15), kind=kOutput, calls=%fused_computation.5 | convolution fusion | flops 805502976 | bytes 5373956 | tf_op jit(solution)/shard_map/dot_general | solution.py:480
  246.9 2.0 combine.2
  248.9 0.0 copy-start.8
  249.0 1.0 copy-done.8
  249.9 0.0 collective-permute-start.14
  250.0 3.4 %combine.3 = (bf16[256,1024]{1,0:T(8,128)(2,1)S(1)}, bf16[256,1024]{1,0:T(8,128)(2,1)S(1)}) custom-call(s32[8]{0:T(128)S(1)} %copy-done.2, f32[4,512]{1,0:T(4,128)S(1)} %copy-done.7, bf16[16,32,2048]{2,1,0:T(8,128)(2,1)} %all-to-all-done.3.result_ref), custom_call_target="tpu_custom_call" | custom-call | flops 2800000000 | bytes 4194304 | tf_op jit(solution)/shard_map/combine/pallas_call | solution.py:258
  253.3 4.8 %collective-permute-start.16 = (bf16[256,1024]{1,0:T(8,128)(2,1)S(1)}, bf16[256,1024]{1,0:T(8,128)(2,1)S(1)}, u32[]{:S(2)}, u32[]{:S(2)}) collective-permute-start(bf16[256,1024]{1,0:T(8,128)(2,1)S(1)} %get-tuple-element.20), channel_id=1, source_target_pairs={{0,4},{1,5},{2,6},{3,7},{4,0},{5,1},{6,2},{7,3},{8,12},{9,13},{10,... | collective-permute-start | bytes 1572872 | tf_op jit(solution)/shard_map/ppermute | solution.py:51
  258.2 0.2 collective-permute-start.17
  258.4 2.9 %fusion.1 = bf16[1536,1024]{1,0:T(8,128)(2,1)} fusion(bf16[1536,1024]{1,0:T(8,128)(2,1)} %fusion.2, s32[]{:T(128)S(6)} %select_n.94, bf16[192,2048]{1,0:T(8,128)(2,1)} %collective-permute-done.5, bf16[2048,1024]{1,0:T(8,128)(2,1)S(1)} %copy-done.16), kind=kOutput, calls=%fused_computation.3 | convolution fusion | flops 805502976 | bytes 5373956 | tf_op jit(solution)/shard_map/dot_general | solution.py:480
  261.3 3.0 %fusion = bf16[1536,1024]{1,0:T(8,128)(2,1)} fusion(bf16[1536,1024]{1,0:T(8,128)(2,1)} %fusion.1, s32[]{:T(128)S(6)} %select_n.95, bf16[192,2048]{1,0:T(8,128)(2,1)} %collective-permute-done.6, bf16[2048,1024]{1,0:T(8,128)(2,1)S(1)} %copy-done.16), kind=kOutput, calls=%fused_computation.1 | convolution fusion | flops 805502976 | bytes 5373956 | tf_op jit(solution)/shard_map/dot_general | solution.py:480
  264.3 4.5 %collective-permute-done.17.diag = bf16[256,1024]{1,0:T(8,128)(2,1)S(1)} collective-permute-done((bf16[256,1024]{1,0:T(8,128)(2,1)S(1)}, bf16[256,1024]{1,0:T(8,128)(2,1)S(1)}, u32[]{:S(2)}, u32[]{:S(2)}) %collective-permute-start.17) | collective-permute-done | bytes 524320 | tf_op jit(solution)/shard_map/ppermute | solution.py:51
  268.8 1.6 total.1
  (48 shorter events, 0.1 us)
Async XLA Ops:
  2.4 16.4 %collective-permute-start.7 = (bf16[256,4096]{1,0:T(8,128)(2,1)S(1)}, bf16[256,4096]{1,0:T(8,128)(2,1)}, u32[]{:S(2)}, u32[]{:S(2)}) collective-permute-start(bf16[256,4096]{1,0:T(8,128)(2,1)S(1)} %constant_dynamic-slice_fusion), channel_id=1, source_target_pairs={{0,4},{1,5},{2,6},{3,7},{4,0},{5,1},{6,2},{7,3},{8,12},{9,13},{10,... | collective-permute-start | bytes 6291464 | tf_op jit(solution)/shard_map/ppermute | solution.py:51
  9.3 8.1 %copy-start.11 = (f32[512,2]{0,1:T(2,128)S(1)}, f32[512,2]{0,1:T(2,128)}, u32[]{:S(2)}) copy-start(f32[512,2]{0,1:T(2,128)} %param.24) | copy-start | bytes 12292
  9.3 8.1 %copy-start.12 = (s32[512,2]{0,1:T(2,128)S(1)}, s32[512,2]{0,1:T(2,128)}, u32[]{:S(2)}) copy-start(s32[512,2]{0,1:T(2,128)} %param.22) | copy-start | bytes 12292
  9.3 8.1 %copy-start.13 = (f32[512]{0:T(512)S(1)}, f32[512]{0:T(512)}, u32[]{:S(2)}) copy-start(f32[512]{0:T(512)} %param.23) | copy-start | bytes 6148
  9.3 41.1 %all-to-all-start = ((bf16[16,32,2048]{2,1,0:T(8,128)(2,1)}), bf16[16,32,2048]{2,1,0:T(8,128)(2,1)}, u32[]{:S(2)}, u32[]{:S(2)}) async-start(bf16[16,32,2048]{2,1,0:T(8,128)(2,1)} %dispatch.2), calls=%async_computation | async-start | bytes 4194304 | tf_op jit(solution)/shard_map/all_to_all | solution.py:55
  17.5 1.3 collective-permute-start.8
  18.8 0.6 copy-start.6
  25.8 29.2 %copy-start.17 = (bf16[1,4096,256]{2,1,0:T(8,128)(2,1)S(1)}, bf16[1,4096,256]{2,1,0:T(8,128)(2,1)}, u32[]{:S(2)}) copy-start(bf16[1,4096,256]{2,1,0:T(8,128)(2,1)} %param.25) | copy-start | bytes 6291460
  50.5 112.1 %all-to-all-start.2 = ((bf16[16,32,4096]{2,1,0:T(8,128)(2,1)}), bf16[16,32,4096]{2,1,0:T(8,128)(2,1)}, u32[]{:S(2)}, u32[]{:S(2)}) async-start(bf16[16,32,4096]{2,1,0:T(8,128)(2,1)} %dispatch.3), calls=%async_computation.2 | async-start | bytes 8388608 | tf_op jit(solution)/shard_map/all_to_all | solution.py:55
  55.0 45.1 %collective-permute-start.10 = (bf16[4096,256]{1,0:T(8,128)(2,1)S(1)}, bf16[4096,256]{1,0:T(8,128)(2,1)S(1)}, u32[]{:S(2)}, u32[]{:S(2)}) collective-permute-start(bf16[4096,256]{1,0:T(8,128)(2,1)S(1)} %bitcast.42), channel_id=1, source_target_pairs={{0,1},{1,0},{2,3},{3,2},{4,7},{5,6},{6,5},{7,4},{8,9},{9,8},{10,11... | collective-permute-start | bytes 6291464 | tf_op jit(solution)/shard_map/ppermute | solution.py:51
  57.6 68.6 %collective-permute-start.11 = (bf16[4096,256]{1,0:T(8,128)(2,1)}, bf16[4096,256]{1,0:T(8,128)(2,1)S(1)}, u32[]{:S(2)}, u32[]{:S(2)}) collective-permute-start(bf16[4096,256]{1,0:T(8,128)(2,1)} %bitcast.43), channel_id=1, source_target_pairs={{0,1},{1,0},{2,3},{3,2},{4,7},{5,6},{6,5},{7,4},{8,9},{9,8},{10,11... | collective-permute-start | bytes 6291464 | tf_op jit(solution)/shard_map/ppermute | solution.py:51
  57.8 69.7 %collective-permute-start.9 = (bf16[512,2048]{1,0:T(8,128)(2,1)}, bf16[512,2048]{1,0:T(8,128)(2,1)}, u32[]{:S(2)}, u32[]{:S(2)}) collective-permute-start(bf16[512,2048]{1,0:T(8,128)(2,1)} %bitcast.14.low), channel_id=1, source_target_pairs={{0,3},{1,2},{2,1},{3,0},{4,5},{5,4},{6,7},{7,6},{8,11},{9,10},{10,... | collective-permute-start | bytes 6291464 | tf_op jit(solution)/shard_map/ppermute | solution.py:51
  57.8 96.9 %collective-permute-start.13 = (bf16[1024,1024]{1,0:T(8,128)(2,1)}, bf16[1024,1024]{1,0:T(8,128)(2,1)}, u32[]{:S(2)}, u32[]{:S(2)}) collective-permute-start(bf16[1024,1024]{1,0:T(8,128)(2,1)} %bitcast.46), channel_id=1, source_target_pairs={{0,1},{1,0},{2,3},{3,2},{4,7},{5,6},{6,5},{7,4},{8,9},{9,8},{10,11... | collective-permute-start | bytes 6291464 | tf_op jit(solution)/shard_map/ppermute | solution.py:51
  100.1 1.3 copy-start.18
  126.1 1.3 copy-start.19
  137.1 17.6 %collective-permute-start.12 = (bf16[512,512]{1,0:T(8,128)(2,1)}, bf16[512,512]{1,0:T(8,128)(2,1)S(1)}, u32[]{:S(2)}, u32[]{:S(2)}) collective-permute-start(bf16[512,512]{1,0:T(8,128)(2,1)} %hidden.2.near), channel_id=1, source_target_pairs={{0,3},{1,2},{2,1},{3,0},{4,5},{5,4},{6,7},{7,6},{8,11},{9,10},{10,... | collective-permute-start | bytes 1572872 | tf_op jit(solution)/shard_map/ppermute | solution.py:51
  138.5 40.4 %collective-permute-start = (bf16[32,2048]{1,0:T(8,128)(2,1)S(1)}, bf16[32,2048]{1,0:T(8,128)(2,1)S(1)}, u32[]{:S(2)}, u32[]{:S(2)}) collective-permute-start(bf16[32,2048]{1,0:T(8,128)(2,1)S(1)} %multiply_convert_fusion), channel_id=1, source_target_pairs={{0,1},{1,2},{2,3},{3,4},{4,5},{5,6},{6,7},{7,8},{8,9},{9,10},{10,1... | collective-permute-start | bytes 393224 | tf_op jit(solution)/shard_map/ppermute | solution.py:436
  154.7 0.8 copy-start.20
  162.6 48.6 %all-to-all-start.1 = ((bf16[16,32,2048]{2,1,0:T(8,128)(2,1)}), bf16[16,32,2048]{2,1,0:T(8,128)(2,1)S(1)}, u32[]{:S(2)}, u32[]{:S(2)}) async-start(bf16[16,32,2048]{2,1,0:T(8,128)(2,1)} %down.2), calls=%async_computation.1 | async-start | bytes 4194304 | tf_op jit(solution)/shard_map/all_to_all | solution.py:55
  169.0 9.9 %copy-start.3 = (f32[31,2048]{1,0:T(8,128)S(1)}, f32[31,2048]{1,0:T(8,128)}, u32[]{:S(2)}) copy-start(f32[31,2048]{1,0:T(8,128)} %taps_ref.1) | copy-start | bytes 761860
  169.0 9.9 %copy-start.4 = (f32[2048]{0:T(1024)S(1)}, f32[2048]{0:T(1024)}, u32[]{:S(2)}) copy-start(f32[2048]{0:T(1024)} %param.17) | copy-start | bytes 24580
  169.0 9.9 %copy-start.5 = (f32[2048]{0:T(1024)S(1)}, f32[2048]{0:T(1024)}, u32[]{:S(2)}) copy-start(f32[2048]{0:T(1024)} %param.18) | copy-start | bytes 24580
  178.9 25.3 %collective-permute-start.15 = (bf16[512,512]{1,0:T(8,128)(2,1)}, bf16[512,512]{1,0:T(8,128)(2,1)}, u32[]{:S(2)}, u32[]{:S(2)}) collective-permute-start(bf16[512,512]{1,0:T(8,128)(2,1)} %hidden.3.near), channel_id=1, source_target_pairs={{0,3},{1,2},{2,1},{3,0},{4,5},{5,4},{6,7},{7,6},{8,11},{9,10},{10,... | collective-permute-start | bytes 1572872 | tf_op jit(solution)/shard_map/ppermute | solution.py:51
  178.9 1.4 copy-start
  180.3 1.4 copy-start.1
  181.8 19.8 %copy-start.14 = (bf16[2048,1024]{1,0:T(8,128)(2,1)S(1)}, bf16[2048,1024]{1,0:T(8,128)(2,1)}, u32[]{:S(2)}) copy-start(bf16[2048,1024]{1,0:T(8,128)(2,1)} %param.19) | copy-start | bytes 12582916
  196.2 36.4 %collective-permute-start.2 = (bf16[192,2048]{1,0:T(8,128)(2,1)}, bf16[192,2048]{1,0:T(8,128)(2,1)}, u32[]{:S(2)}, u32[]{:S(2)}) collective-permute-start(bf16[192,2048]{1,0:T(8,128)(2,1)} %get-tuple-element.15), channel_id=1, source_target_pairs={{0,3},{1,0},{2,1},{3,2},{4,7},{5,4},{6,5},{7,6},{8,11},{9,8},{10,9... | collective-permute-start | bytes 2359304 | tf_op jit(solution)/shard_map/ppermute | solution.py:461
  198.5 42.6 %collective-permute-start.3 = (bf16[192,2048]{1,0:T(8,128)(2,1)}, bf16[192,2048]{1,0:T(8,128)(2,1)}, u32[]{:S(2)}, u32[]{:S(2)}) collective-permute-start(bf16[192,2048]{1,0:T(8,128)(2,1)} %get-tuple-element.15), channel_id=1, source_target_pairs={{0,1},{1,2},{2,3},{3,0},{4,5},{5,6},{6,7},{7,4},{8,9},{9,10},{10,1... | collective-permute-start | bytes 2359304 | tf_op jit(solution)/shard_map/ppermute | solution.py:461
  198.5 34.1 %collective-permute-start.1 = (bf16[192,2048]{1,0:T(8,128)(2,1)S(1)}, bf16[192,2048]{1,0:T(8,128)(2,1)}, u32[]{:S(2)}, u32[]{:S(2)}) collective-permute-start(bf16[192,2048]{1,0:T(8,128)(2,1)S(1)} %get-tuple-element.14), channel_id=1, source_target_pairs={{0,1},{1,2},{2,3},{3,0},{4,5},{5,6},{6,7},{7,4},{8,9},{9,10},{10,1... | collective-permute-start | bytes 2359304 | tf_op jit(solution)/shard_map/ppermute | solution.py:461
  199.3 44.7 %collective-permute-start.4 = (bf16[192,2048]{1,0:T(8,128)(2,1)S(1)}, bf16[192,2048]{1,0:T(8,128)(2,1)}, u32[]{:S(2)}, u32[]{:S(2)}) collective-permute-start(bf16[192,2048]{1,0:T(8,128)(2,1)S(1)} %get-tuple-element.14), channel_id=1, source_target_pairs={{0,3},{1,0},{2,1},{3,2},{4,7},{5,4},{6,5},{7,6},{8,11},{9,8},{10,9... | collective-permute-start | bytes 2359304 | tf_op jit(solution)/shard_map/ppermute | solution.py:461
  202.6 1.7 copy-start.10
  211.2 38.8 %all-to-all-start.3 = ((bf16[16,32,2048]{2,1,0:T(8,128)(2,1)}), bf16[16,32,2048]{2,1,0:T(8,128)(2,1)}, u32[]{:S(2)}, u32[]{:S(2)}) async-start(bf16[16,32,2048]{2,1,0:T(8,128)(2,1)} %down.3), calls=%async_computation.3 | async-start | bytes 4194304 | tf_op jit(solution)/shard_map/all_to_all | solution.py:55
  217.9 17.4 %copy-start.15 = (bf16[2048,1024]{1,0:T(8,128)(2,1)S(1)}, bf16[2048,1024]{1,0:T(8,128)(2,1)}, u32[]{:S(2)}) copy-start(bf16[2048,1024]{1,0:T(8,128)(2,1)} %param.19) | copy-start | bytes 12582916
  232.6 25.8 %collective-permute-start.5 = (bf16[192,2048]{1,0:T(8,128)(2,1)}, bf16[192,2048]{1,0:T(8,128)(2,1)}, u32[]{:S(2)}, u32[]{:S(2)}) collective-permute-start(bf16[192,2048]{1,0:T(8,128)(2,1)} %collective-permute-done.1), channel_id=1, source_target_pairs={{0,1},{1,2},{2,3},{3,0},{4,5},{5,6},{6,7},{7,4},{8,9},{9,10},{10,1... | collective-permute-start | bytes 2359304 | tf_op jit(solution)/shard_map/ppermute | solution.py:461
  232.6 28.7 %collective-permute-start.6 = (bf16[192,2048]{1,0:T(8,128)(2,1)}, bf16[192,2048]{1,0:T(8,128)(2,1)}, u32[]{:S(2)}, u32[]{:S(2)}) collective-permute-start(bf16[192,2048]{1,0:T(8,128)(2,1)} %collective-permute-done.2), channel_id=1, source_target_pairs={{0,3},{1,0},{2,1},{3,2},{4,7},{5,4},{6,5},{7,6},{8,11},{9,8},{10,9... | collective-permute-start | bytes 2359304 | tf_op jit(solution)/shard_map/ppermute | solution.py:461
  244.0 2.9 %copy-start.2 = (s32[8]{0:T(128)S(1)}, s32[8]{0:T(128)}, u32[]{:S(2)}) copy-start(s32[8]{0:T(128)} %stack.43.where) | copy-start | bytes 100
  246.9 3.0 %copy-start.7 = (f32[4,512]{1,0:T(4,128)S(1)}, f32[4,512]{1,0:T(4,128)}, u32[]{:S(2)}) copy-start(f32[4,512]{1,0:T(4,128)} %copy-done.6) | copy-start | bytes 24580
  248.9 1.0 copy-start.8
  249.9 14.4 %collective-permute-start.14 = (bf16[256,1024]{1,0:T(8,128)(2,1)S(1)}, bf16[256,1024]{1,0:T(8,128)(2,1)S(1)}, u32[]{:S(2)}, u32[]{:S(2)}) collective-permute-start(bf16[256,1024]{1,0:T(8,128)(2,1)S(1)} %get-tuple-element.18), channel_id=1, source_target_pairs={{0,1},{1,0},{2,3},{3,2},{4,7},{5,6},{6,5},{7,4},{8,9},{9,8},{10,11... | collective-permute-start | bytes 1572872 | tf_op jit(solution)/shard_map/ppermute | solution.py:51
  250.0 8.4 %copy-start.16 = (bf16[2048,1024]{1,0:T(8,128)(2,1)S(1)}, bf16[2048,1024]{1,0:T(8,128)(2,1)}, u32[]{:S(2)}) copy-start(bf16[2048,1024]{1,0:T(8,128)(2,1)} %param.19) | copy-start | bytes 12582916
  253.3 11.0 %collective-permute-start.16 = (bf16[256,1024]{1,0:T(8,128)(2,1)S(1)}, bf16[256,1024]{1,0:T(8,128)(2,1)S(1)}, u32[]{:S(2)}, u32[]{:S(2)}) collective-permute-start(bf16[256,1024]{1,0:T(8,128)(2,1)S(1)} %get-tuple-element.20), channel_id=1, source_target_pairs={{0,4},{1,5},{2,6},{3,7},{4,0},{5,1},{6,2},{7,3},{8,12},{9,13},{10,... | collective-permute-start | bytes 1572872 | tf_op jit(solution)/shard_map/ppermute | solution.py:51
  258.2 10.6 %collective-permute-start.17 = (bf16[256,1024]{1,0:T(8,128)(2,1)S(1)}, bf16[256,1024]{1,0:T(8,128)(2,1)S(1)}, u32[]{:S(2)}, u32[]{:S(2)}) collective-permute-start(bf16[256,1024]{1,0:T(8,128)(2,1)S(1)} %get-tuple-element.21), channel_id=1, source_target_pairs={{0,5},{1,4},{2,7},{3,6},{4,3},{5,2},{6,1},{7,0},{8,13},{9,12},{10,... | collective-permute-start | bytes 1572872 | tf_op jit(solution)/shard_map/ppermute | solution.py:51
  261.3 7.5 %copy-start.9 = (f32[256,1024]{1,0:T(8,128)S(1)}, f32[256,1024]{1,0:T(8,128)}, u32[]{:S(2)}) copy-start(f32[256,1024]{1,0:T(8,128)} %copy-done.8) | copy-start | bytes 3145732

commit v3 on v2

--- a/solution.py
+++ b/solution.py
@@ -185,11 +185,12 @@
         ),
         out_shape=jax.ShapeDtypeStruct((rows, 2 * width), bf16),
         cost_estimate=cost(10, 12),
+        compiler_params=params(60 if low is high else 24),
         name="hidden",
     )(where, low, high, gate_own, up_own, gate_part, up_part)
 
 
-def down_kernel(where, near, far, own_ref, part_ref, out_ref):
+def down_kernel(where, near, far, own_ref, part_a, part_b, out_ref):
     quarter = near.shape[1] // 2
 
     def run(weight):
@@ -206,12 +207,16 @@
     def _():
         run(own_ref)
 
-    @pl.when(pl.program_id(0) >= 2)
-    def _():
-        run(part_ref)
-
-
-def down_result(where, near, far, down_own, down_part):
+    @pl.when(pl.program_id(0) == 2)
+    def _():
+        run(part_a)
+
+    @pl.when(pl.program_id(0) == 3)
+    def _():
+        run(part_b)
+
+
+def down_result(where, near, far, down_own, down_a, down_b):
     rows = near.shape[0]
     depth, width = down_own.shape
     step = width // 2
@@ -225,14 +230,16 @@
                 whole,
                 whole,
                 pl.BlockSpec((depth, step), lambda j, w: (0, jnp.minimum(j, 1))),
-                pl.BlockSpec((depth, step), lambda j, w: (0, jnp.maximum(j - 2, 0))),
+                pl.BlockSpec((depth, step), lambda j, w: (0, 0)),
+                pl.BlockSpec((depth, step), lambda j, w: (0, 0)),
             ],
             out_specs=pl.BlockSpec((PLANES, rows // PLANES, step), lambda j, w: (0, 0, j)),
         ),
         out_shape=jax.ShapeDtypeStruct((PLANES, rows // PLANES, 2 * width), bf16),
         cost_estimate=cost(5, 7),
+        compiler_params=params(20),
         name="down",
-    )(where, near, far, down_own, down_part)
+    )(where, near, far, down_own, down_a, down_b)
 
 
 def combine_kernel(where, info_ref, result_ref, own_slice, other_slice):
@@ -438,13 +445,15 @@
     top, bottom = conv_rows(
         conv_value, conv_gate, earlier, conv_taps, conv_gain, conv_bias
     )
-    down_part = swapped(down_own, weight_partner)
+    middle_out = down_own.shape[1] // 2
+    down_a = swapped(down_own[:, :middle_out], weight_partner)
+    down_b = swapped(down_own[:, middle_out:], weight_partner)
 
     combined = []
     for k in range(CHUNKS):
         near = hidden_units(where, *arrived[k], gate_own, up_own, gate_part, up_part)
         far = swapped(near, hidden_partner)
-        result = down_result(where, near, far, down_own, down_part)
+        result = down_result(where, near, far, down_own, down_a, down_b)
         returned = exchanged(result)
         combined.append(combine(where, infos[k], returned, (f32, bf16)[k]))
     keep, from_partner = combined[0][0], swapped(combined[0][1], weight_partner)

time: 271 us -> 273 us (level)
  Pallas kernels: 66.2 us -> 60.9 us
  waiting for transfers between devices: 118 us -> 123 us
    ppermute x11 -> x12, waiting for transfers between devices: 83 us -> 88 us  [swapped(): return lax.ppermute(value, CORE_TP, ring_pairs(move))]
    pallas_call x2, Pallas kernels: 14 us -> 10.3 us  [down_result(): pl.pallas_call(down_kernel, grid_spec=pltpu.PrefetchScalarGridSpec(num_sc...]
    ppermute x11 -> x12, starting transfers between devices: 12.5 us -> 11.6 us  [swapped(): return lax.ppermute(value, CORE_TP, ring_pairs(move))]
    unnamed x42 -> x52, local copies, waits for them, and re-layouts: 9.53 us -> 8.79 us
  transfers between devices with their start and end apart: 22 -> 23, of which waited for: 7 -> 7; matrix products, arithmetic and copies ran while one was open for 9% -> 10% of each run, Pallas kernels for 24% -> 22%
where the time goes in v3:
time: 273 us; the launch traced here: 272 us
  waiting for transfers between devices  123 us (45%)
  Pallas kernels  60.9 us (22%)
  starting transfers between devices  48 us (18%)
  matrix products  24 us (9%)
  local copies, waits for them, and re-layouts  13 us (5%)
    ppermute x12, waiting for transfers between devices, swapped(): return lax.ppermute(value, CORE_TP, ring_pairs(move))  88 us
    all_to_all x4, starting transfers between devices, exchanged(): lax.all_to_all(blocks, CHIPS, split_axis=0, concat_axis=0, tiled=True)  26 us
    all_to_all x4, waiting for transfers between devices, exchanged(): lax.all_to_all(blocks, CHIPS, split_axis=0, concat_axis=0, tiled=True)  24.7 us
    dot_general x8, matrix products, work(): jnp.dot(block, conv_projection, preferred_element_type=f32).astype(bf16)  24 us
    pallas_call x2, Pallas kernels, hidden_units(): pl.pallas_call(hidden_kernel, grid_spec=pltpu.PrefetchScalarGridSpec(num_...  18.1 us
    pallas_call x1, Pallas kernels, conv_rows(): pl.pallas_call(conv_kernel, grid=(length // block,), in_specs=[row_block,...  14.6 us
    ppermute x12, starting transfers between devices, swapped(): return lax.ppermute(value, CORE_TP, ring_pairs(move))  11.6 us
    pallas_call x2, Pallas kernels, dispatch(): pl.pallas_call(dispatch_kernel, grid_spec=pltpu.PrefetchScalarGridSpec(nu...  11.2 us
  transfers between devices with their start and end apart: 23, of which 7 were waited for; matrix products, arithmetic and copies ran while one was open for 10% of the time, Pallas kernels for 22%

profile of v3, /device:TPU:1, one launch (start us, length us, event | category | flops | bytes accessed | tf_op | source)
XLA Modules:
  0.0 271.6 jit_solution(12599496812822972432)
XLA Ops:
  0.7 1.7 constant_dynamic-slice_fusion
  2.4 1.5 collective-permute-start.7
  3.9 0.6 stack.43.where
  4.5 4.8 %dispatch.2 = bf16[16,32,2048]{2,1,0:T(8,128)(2,1)} custom-call(s32[8]{0:T(128)} %stack.43.where, bf16[512,4096]{1,0:T(8,128)(2,1)} %x_ref.1, s32[2,512]{1,0:T(2,128)} %bitcast.48, f32[1,4096]{1,0:T(1,128)} %bitcast.49), custom_call_target="tpu_custom_call" | custom-call | flops 4200000000 | bytes 6291456 | tf_op jit(solution)/shard_map/dispatch/pallas_call | solution.py:116
  9.3 8.1 %all-to-all-start = ((bf16[16,32,2048]{2,1,0:T(8,128)(2,1)}), bf16[16,32,2048]{2,1,0:T(8,128)(2,1)}, u32[]{:S(2)}, u32[]{:S(2)}) async-start(bf16[16,32,2048]{2,1,0:T(8,128)(2,1)} %dispatch.2), calls=%async_computation | async-start | bytes 4194304 | tf_op jit(solution)/shard_map/all_to_all | solution.py:55
  17.4 0.5 collective-permute-start.8
  17.9 0.8 collective-permute-done.8.info_ref
  18.8 0.6 copy-done.15
  19.3 6.4 %dispatch.3 = bf16[16,32,4096]{2,1,0:T(8,128)(2,1)} custom-call(s32[8]{0:T(128)} %stack.43.where, bf16[256,4096]{1,0:T(8,128)(2,1)} %collective-permute-done.7.x_ref, f32[4,512]{1,0:T(4,128)} %copy-done.15, f32[1,4096]{1,0:T(1,128)} %bitcast.50), custom_call_target="tpu_custom_call" | custom-call | flops 4200000000 | bytes 6291456 | tf_op jit(solution)/shard_map/dispatch/pallas_call | solution.py:116
  25.7 24.7 %all-to-all-done = bf16[16,32,2048]{2,1,0:T(8,128)(2,1)} async-done(((bf16[16,32,2048]{2,1,0:T(8,128)(2,1)}), bf16[16,32,2048]{2,1,0:T(8,128)(2,1)}, u32[]{:S(2)}, u32[]{:S(2)}) %all-to-all-start) | async-done | bytes 2097184 | tf_op jit(solution)/shard_map/all_to_all | solution.py:55
  50.4 4.5 %all-to-all-start.2 = ((bf16[16,32,4096]{2,1,0:T(8,128)(2,1)}), bf16[16,32,4096]{2,1,0:T(8,128)(2,1)}, u32[]{:S(2)}, u32[]{:S(2)}) async-start(bf16[16,32,4096]{2,1,0:T(8,128)(2,1)} %dispatch.3), calls=%async_computation.2 | async-start | bytes 8388608 | tf_op jit(solution)/shard_map/all_to_all | solution.py:55
  54.9 0.0 copy-start.7
  55.0 0.0 copy-start.8
  55.0 2.6 collective-permute-start.10
  57.5 0.2 collective-permute-start.11
  57.7 0.0 collective-permute-start.9
  57.7 1.5 fusion.8
  59.2 2.5 collective-permute-start.13
  61.7 0.2 collective-permute-start.14
  61.9 38.6 %collective-permute-done.10.gate_part = bf16[4096,256]{1,0:T(8,128)(2,1)S(1)} collective-permute-done((bf16[4096,256]{1,0:T(8,128)(2,1)}, bf16[4096,256]{1,0:T(8,128)(2,1)S(1)}, u32[]{:S(2)}, u32[]{:S(2)}) %collective-permute-start.10) | collective-permute-done | bytes 2097184 | tf_op jit(solution)/shard_map/ppermute | solution.py:51
  100.5 25.8 %collective-permute-done.11.up_part = bf16[4096,256]{1,0:T(8,128)(2,1)S(1)} collective-permute-done((bf16[4096,256]{1,0:T(8,128)(2,1)}, bf16[4096,256]{1,0:T(8,128)(2,1)S(1)}, u32[]{:S(2)}, u32[]{:S(2)}) %collective-permute-start.11) | collective-permute-done | bytes 2097184 | tf_op jit(solution)/shard_map/ppermute | solution.py:51
  126.3 8.3 %hidden.2.near = bf16[512,512]{1,0:T(8,128)(2,1)} custom-call(s32[8]{0:T(128)S(1)} %copy-done.5, bf16[512,2048]{1,0:T(8,128)(2,1)} %bitcast.14.low, bf16[512,2048]{1,0:T(8,128)(2,1)S(1)} %collective-permute-done.9.high, bf16[4096,256]{1,0:T(8,128)(2,1)S(1)} %bitcast.42, bf16[4096,256]{1,0:T(8,128)(2,1)S(1)} %bitcast.45, ...), custom_call_target="tpu_custom_call" | custom-call | flops 7000000000 | bytes 12582912 | tf_op jit(solution)/shard_map/hidden/pallas_call | solution.py:173
  134.6 0.3 collective-permute-start.12
  134.9 1.0 multiply_convert_fusion
  136.0 3.1 %collective-permute-start = (bf16[32,2048]{1,0:T(8,128)(2,1)S(1)}, bf16[32,2048]{1,0:T(8,128)(2,1)S(1)}, u32[]{:S(2)}, u32[]{:S(2)}) collective-permute-start(bf16[32,2048]{1,0:T(8,128)(2,1)S(1)} %multiply_convert_fusion), channel_id=1, source_target_pairs={{0,1},{1,2},{2,3},{3,4},{4,5},{5,6},{6,7},{7,8},{8,9},{9,10},{10,1... | collective-permute-start | bytes 393224 | tf_op jit(solution)/shard_map/ppermute | solution.py:443
  139.1 16.8 %collective-permute-done.14.part_b = bf16[1024,512]{1,0:T(8,128)(2,1)} collective-permute-done((bf16[1024,512]{1,0:T(8,128)(2,1)}, bf16[1024,512]{1,0:T(8,128)(2,1)}, u32[]{:S(2)}, u32[]{:S(2)}) %collective-permute-start.14) | collective-permute-done | bytes 1048608 | tf_op jit(solution)/shard_map/ppermute | solution.py:51
  155.9 5.3 %down.2 = bf16[16,32,2048]{2,1,0:T(8,128)(2,1)S(1)} custom-call(s32[8]{0:T(128)S(1)} %copy-done.5, bf16[512,512]{1,0:T(8,128)(2,1)} %hidden.2.near, bf16[512,512]{1,0:T(8,128)(2,1)} %collective-permute-done.12.far, bf16[1024,1024]{1,0:T(8,128)(2,1)S(1)} %bitcast.38, bf16[1024,512]{1,0:T(8,128)(2,1)S(1)} %collective-permute-done.13.part_a, ...), custom_call_target="tpu_custom_call" | custom-call | flops 3500000000 | bytes 7340032 | tf_op jit(solution)/shard_map/down/pallas_call | solution.py:224
  161.2 1.3 copy-done.2
  162.5 6.8 %all-to-all-start.1 = ((bf16[16,32,2048]{2,1,0:T(8,128)(2,1)}), bf16[16,32,2048]{2,1,0:T(8,128)(2,1)}, u32[]{:S(2)}, u32[]{:S(2)}) async-start(bf16[16,32,2048]{2,1,0:T(8,128)(2,1)} %copy-done.2), calls=%async_computation.1 | async-start | bytes 4194304 | tf_op jit(solution)/shard_map/all_to_all | solution.py:55
  169.3 0.0 copy-start.12
  169.3 0.0 copy-start.13
  169.3 0.0 copy-start.14
  169.3 9.8 %hidden.3.near = bf16[512,512]{1,0:T(8,128)(2,1)} custom-call(s32[8]{0:T(128)} %stack.43.where, bf16[512,4096]{1,0:T(8,128)(2,1)} %bitcast.18.low.high, bf16[512,4096]{1,0:T(8,128)(2,1)} %bitcast.18.low.high, bf16[4096,256]{1,0:T(8,128)(2,1)} %bitcast.41, bf16[4096,256]{1,0:T(8,128)(2,1)} %bitcast.44, bf16[4096,256]{1,0:T(8,128)(2,1)} %copy-done.9, ...), custom_call_target="tpu_custom_call" | custom-call | flops 7000000000 | bytes 12582912 | tf_op jit(solution)/shard_map/hidden/pallas_call | solution.py:173
  179.2 0.0 copy-start.3
  179.2 1.4 copy-done.3
  180.6 1.4 copy-done.4
  182.0 14.6 %shard_map.149 = (bf16[192,2048]{1,0:T(8,128)(2,1)}, bf16[192,2048]{1,0:T(8,128)(2,1)}) custom-call(bf16[384,2048]{1,0:T(8,128)(2,1)S(1)} %copy-done.3, bf16[384,2048]{1,0:T(8,128)(2,1)S(1)} %copy-done.4, bf16[32,2048]{1,0:T(8,128)(2,1)S(1)} %collective-permute-done.halo_ref, f32[31,2048]{1,0:T(8,128)S(1)} %copy-done.12, f32[1,2048]{1,0:T(1,128)S(1)} %bitcast.46, ...), custom_call_target="tpu_custom_call" | custom-call | flops 9799999488 | bytes 5242880 | tf_op jit(solution)/shard_map/pallas_call | solution.py:372
  196.6 1.9 collective-permute-start.2
  198.5 1.0 collective-permute-start.1
  199.5 1.7 collective-permute-start.4
  201.2 0.4 broadcast_in_dim.14
  201.6 2.2 fusion.7
  203.8 0.0 copy-start.19
  203.9 1.6 copy-done.19
  205.5 5.0 %down.3 = bf16[16,32,2048]{2,1,0:T(8,128)(2,1)S(1)} custom-call(s32[8]{0:T(128)S(1)} %copy-done.6, bf16[512,512]{1,0:T(8,128)(2,1)S(1)} %copy-done.11, bf16[512,512]{1,0:T(8,128)(2,1)S(1)} %collective-permute-done.16.far, bf16[1024,1024]{1,0:T(8,128)(2,1)S(1)} %bitcast.39, bf16[1024,512]{1,0:T(8,128)(2,1)S(1)} %collective-permute-done.13.part_a, ...), custom_call_target="tpu_custom_call" | custom-call | flops 3500000000 | bytes 7340032 | tf_op jit(solution)/shard_map/down/pallas_call | solution.py:224
  210.5 1.4 copy-done.1
  211.9 6.6 %all-to-all-start.3 = ((bf16[16,32,2048]{2,1,0:T(8,128)(2,1)}), bf16[16,32,2048]{2,1,0:T(8,128)(2,1)S(1)}, u32[]{:S(2)}, u32[]{:S(2)}) async-start(bf16[16,32,2048]{2,1,0:T(8,128)(2,1)} %copy-done.1), calls=%async_computation.3 | async-start | bytes 4194304 | tf_op jit(solution)/shard_map/all_to_all | solution.py:55
  218.5 0.0 copy-start.24
  218.5 4.3 %fusion.6 = bf16[1536,1024]{1,0:T(8,128)(2,1)} fusion(bf16[1536,1024]{1,0:T(8,128)(2,1)} %copy-done.19, s32[]{:T(128)S(6)} %select_n.86, bf16[192,2048]{1,0:T(8,128)(2,1)} %get-tuple-element.15, bf16[2048,1024]{1,0:T(8,128)(2,1)} %param.19), kind=kOutput, calls=%fused_computation.13 | convolution fusion | flops 805502976 | bytes 5373956 | tf_op jit(solution)/shard_map/dot_general | solution.py:489
  222.8 10.8 %collective-permute-done.1 = bf16[192,2048]{1,0:T(8,128)(2,1)} collective-permute-done((bf16[192,2048]{1,0:T(8,128)(2,1)}, bf16[192,2048]{1,0:T(8,128)(2,1)}, u32[]{:S(2)}, u32[]{:S(2)}) %collective-permute-start.1) | collective-permute-done | bytes 786464 | tf_op jit(solution)/shard_map/ppermute | solution.py:470
  233.6 2.7 collective-permute-start.6
  236.3 2.9 %fusion.5 = bf16[1536,1024]{1,0:T(8,128)(2,1)} fusion(bf16[1536,1024]{1,0:T(8,128)(2,1)} %fusion.6, s32[]{:T(128)S(6)} %select_n.88, bf16[192,2048]{1,0:T(8,128)(2,1)} %collective-permute-done.1, bf16[2048,1024]{1,0:T(8,128)(2,1)S(1)} %copy-done.24), kind=kOutput, calls=%fused_computation.11 | convolution fusion | flops 805502976 | bytes 5373956 | tf_op jit(solution)/shard_map/dot_general | solution.py:489
  239.2 2.9 %fusion.4 = bf16[1536,1024]{1,0:T(8,128)(2,1)} fusion(bf16[1536,1024]{1,0:T(8,128)(2,1)} %fusion.5, s32[]{:T(128)S(6)} %select_n.90, bf16[192,2048]{1,0:T(8,128)(2,1)} %collective-permute-done.2, bf16[2048,1024]{1,0:T(8,128)(2,1)S(1)} %copy-done.24), kind=kOutput, calls=%fused_computation.9 | convolution fusion | flops 805502976 | bytes 5373956 | tf_op jit(solution)/shard_map/dot_general | solution.py:489
  242.1 2.9 %fusion.3 = bf16[1536,1024]{1,0:T(8,128)(2,1)} fusion(bf16[1536,1024]{1,0:T(8,128)(2,1)} %fusion.4, s32[]{:T(128)S(6)} %select_n.91, bf16[192,2048]{1,0:T(8,128)(2,1)} %collective-permute-done.3, bf16[2048,1024]{1,0:T(8,128)(2,1)S(1)} %copy-done.24), kind=kOutput, calls=%fused_computation.7 | convolution fusion | flops 805502976 | bytes 5373956 | tf_op jit(solution)/shard_map/dot_general | solution.py:489
  245.0 2.9 %fusion.2 = bf16[1536,1024]{1,0:T(8,128)(2,1)} fusion(bf16[1536,1024]{1,0:T(8,128)(2,1)} %fusion.3, s32[]{:T(128)S(6)} %select_n.92, bf16[192,2048]{1,0:T(8,128)(2,1)} %collective-permute-done.4, bf16[2048,1024]{1,0:T(8,128)(2,1)S(1)} %copy-done.24), kind=kOutput, calls=%fused_computation.5 | convolution fusion | flops 805502976 | bytes 5373956 | tf_op jit(solution)/shard_map/dot_general | solution.py:489
  247.9 3.1 %combine.2 = (f32[256,1024]{1,0:T(8,128)S(1)}, bf16[256,1024]{1,0:T(8,128)(2,1)S(1)}) custom-call(s32[8]{0:T(128)S(1)} %copy-done.6, f32[4,512]{1,0:T(4,128)S(1)} %pad_maximum_fusion.info_ref, bf16[16,32,2048]{2,1,0:T(8,128)(2,1)} %all-to-all-done.1.result_ref), custom_call_target="tpu_custom_call" | custom-call | flops 2800000000 | bytes 4194304 | tf_op jit(solution)/shard_map/combine/pallas_call | solution.py:265
  251.0 1.0 copy-done.17
  252.0 0.0 collective-permute-start.15
  252.0 2.0 combine.3
  254.1 3.9 %collective-permute-start.17 = (bf16[256,1024]{1,0:T(8,128)(2,1)S(1)}, bf16[256,1024]{1,0:T(8,128)(2,1)S(1)}, u32[]{:S(2)}, u32[]{:S(2)}) collective-permute-start(bf16[256,1024]{1,0:T(8,128)(2,1)S(1)} %get-tuple-element.20), channel_id=1, source_target_pairs={{0,4},{1,5},{2,6},{3,7},{4,0},{5,1},{6,2},{7,3},{8,12},{9,13},{10,... | collective-permute-start | bytes 1572872 | tf_op jit(solution)/shard_map/ppermute | solution.py:51
  257.9 2.9 %fusion.1 = bf16[1536,1024]{1,0:T(8,128)(2,1)} fusion(bf16[1536,1024]{1,0:T(8,128)(2,1)} %fusion.2, s32[]{:T(128)S(6)} %select_n.94, bf16[192,2048]{1,0:T(8,128)(2,1)} %collective-permute-done.5, bf16[2048,1024]{1,0:T(8,128)(2,1)S(1)} %copy-done.25), kind=kOutput, calls=%fused_computation.3 | convolution fusion | flops 805502976 | bytes 5373956 | tf_op jit(solution)/shard_map/dot_general | solution.py:489
  260.9 3.0 %fusion = bf16[1536,1024]{1,0:T(8,128)(2,1)} fusion(bf16[1536,1024]{1,0:T(8,128)(2,1)} %fusion.1, s32[]{:T(128)S(6)} %select_n.95, bf16[192,2048]{1,0:T(8,128)(2,1)} %collective-permute-done.6, bf16[2048,1024]{1,0:T(8,128)(2,1)S(1)} %copy-done.25), kind=kOutput, calls=%fused_computation.1 | convolution fusion | flops 805502976 | bytes 5373956 | tf_op jit(solution)/shard_map/dot_general | solution.py:489
  263.9 6.0 %collective-permute-done.18.diag = bf16[256,1024]{1,0:T(8,128)(2,1)S(1)} collective-permute-done((bf16[256,1024]{1,0:T(8,128)(2,1)S(1)}, bf16[256,1024]{1,0:T(8,128)(2,1)S(1)}, u32[]{:S(2)}, u32[]{:S(2)}) %collective-permute-start.18) | collective-permute-done | bytes 524320 | tf_op jit(solution)/shard_map/ppermute | solution.py:51
  269.9 1.6 total.1
  (61 shorter events, 0.2 us)
Async XLA Ops:
  2.4 16.4 %collective-permute-start.7 = (bf16[256,4096]{1,0:T(8,128)(2,1)S(1)}, bf16[256,4096]{1,0:T(8,128)(2,1)}, u32[]{:S(2)}, u32[]{:S(2)}) collective-permute-start(bf16[256,4096]{1,0:T(8,128)(2,1)S(1)} %constant_dynamic-slice_fusion), channel_id=1, source_target_pairs={{0,4},{1,5},{2,6},{3,7},{4,0},{5,1},{6,2},{7,3},{8,12},{9,13},{10,... | collective-permute-start | bytes 6291464 | tf_op jit(solution)/shard_map/ppermute | solution.py:51
  9.3 8.1 %copy-start.20 = (f32[512,2]{0,1:T(2,128)S(1)}, f32[512,2]{0,1:T(2,128)}, u32[]{:S(2)}) copy-start(f32[512,2]{0,1:T(2,128)} %param.24) | copy-start | bytes 12292
  9.3 8.1 %copy-start.21 = (s32[512,2]{0,1:T(2,128)S(1)}, s32[512,2]{0,1:T(2,128)}, u32[]{:S(2)}) copy-start(s32[512,2]{0,1:T(2,128)} %param.22) | copy-start | bytes 12292
  9.3 8.1 %copy-start.22 = (f32[512]{0:T(512)S(1)}, f32[512]{0:T(512)}, u32[]{:S(2)}) copy-start(f32[512]{0:T(512)} %param.23) | copy-start | bytes 6148
  9.3 41.1 %all-to-all-start = ((bf16[16,32,2048]{2,1,0:T(8,128)(2,1)}), bf16[16,32,2048]{2,1,0:T(8,128)(2,1)}, u32[]{:S(2)}, u32[]{:S(2)}) async-start(bf16[16,32,2048]{2,1,0:T(8,128)(2,1)} %dispatch.2), calls=%async_computation | async-start | bytes 4194304 | tf_op jit(solution)/shard_map/all_to_all | solution.py:55
  17.4 1.3 collective-permute-start.8
  18.7 0.6 copy-start.15
  25.7 32.0 %copy-start = (bf16[1,1024,1024]{2,1,0:T(8,128)(2,1)S(1)}, bf16[1,1024,1024]{2,1,0:T(8,128)(2,1)}, u32[]{:S(2)}) copy-start(bf16[1,1024,1024]{2,1,0:T(8,128)(2,1)} %param.27) | copy-start | bytes 6291460
  50.4 112.2 %all-to-all-start.2 = ((bf16[16,32,4096]{2,1,0:T(8,128)(2,1)}), bf16[16,32,4096]{2,1,0:T(8,128)(2,1)}, u32[]{:S(2)}, u32[]{:S(2)}) async-start(bf16[16,32,4096]{2,1,0:T(8,128)(2,1)} %dispatch.3), calls=%async_computation.2 | async-start | bytes 8388608 | tf_op jit(solution)/shard_map/all_to_all | solution.py:55
  54.9 71.4 %copy-start.5 = (s32[8]{0:T(128)S(1)}, s32[8]{0:T(128)}, u32[]{:S(2)}) copy-start(s32[8]{0:T(128)} %stack.43.where) | copy-start | bytes 100
  54.9 71.4 %copy-start.7 = (bf16[1,4096,256]{2,1,0:T(8,128)(2,1)S(1)}, bf16[1,4096,256]{2,1,0:T(8,128)(2,1)}, u32[]{:S(2)}) copy-start(bf16[1,4096,256]{2,1,0:T(8,128)(2,1)} %param.25) | copy-start | bytes 6291460
  55.0 71.4 %copy-start.8 = (bf16[1,4096,256]{2,1,0:T(8,128)(2,1)S(1)}, bf16[1,4096,256]{2,1,0:T(8,128)(2,1)}, u32[]{:S(2)}) copy-start(bf16[1,4096,256]{2,1,0:T(8,128)(2,1)} %param.26) | copy-start | bytes 6291460
  55.0 45.5 %collective-permute-start.10 = (bf16[4096,256]{1,0:T(8,128)(2,1)}, bf16[4096,256]{1,0:T(8,128)(2,1)S(1)}, u32[]{:S(2)}, u32[]{:S(2)}) collective-permute-start(bf16[4096,256]{1,0:T(8,128)(2,1)} %bitcast.40), channel_id=1, source_target_pairs={{0,1},{1,0},{2,3},{3,2},{4,7},{5,6},{6,5},{7,4},{8,9},{9,8},{10,11... | collective-permute-start | bytes 6291464 | tf_op jit(solution)/shard_map/ppermute | solution.py:51
  57.5 68.8 %collective-permute-start.11 = (bf16[4096,256]{1,0:T(8,128)(2,1)}, bf16[4096,256]{1,0:T(8,128)(2,1)S(1)}, u32[]{:S(2)}, u32[]{:S(2)}) collective-permute-start(bf16[4096,256]{1,0:T(8,128)(2,1)} %bitcast.43), channel_id=1, source_target_pairs={{0,1},{1,0},{2,3},{3,2},{4,7},{5,6},{6,5},{7,4},{8,9},{9,8},{10,11... | collective-permute-start | bytes 6291464 | tf_op jit(solution)/shard_map/ppermute | solution.py:51
  57.7 68.6 %collective-permute-start.9 = (bf16[512,2048]{1,0:T(8,128)(2,1)}, bf16[512,2048]{1,0:T(8,128)(2,1)S(1)}, u32[]{:S(2)}, u32[]{:S(2)}) collective-permute-start(bf16[512,2048]{1,0:T(8,128)(2,1)} %bitcast.14.low), channel_id=1, source_target_pairs={{0,3},{1,2},{2,1},{3,0},{4,5},{5,4},{6,7},{7,6},{8,11},{9,10},{10,... | collective-permute-start | bytes 6291464 | tf_op jit(solution)/shard_map/ppermute | solution.py:51
  59.2 79.9 %collective-permute-start.13 = (bf16[1024,512]{1,0:T(8,128)(2,1)}, bf16[1024,512]{1,0:T(8,128)(2,1)S(1)}, u32[]{:S(2)}, u32[]{:S(2)}) collective-permute-start(bf16[1024,512]{1,0:T(8,128)(2,1)} %get-tuple-element.23), channel_id=1, source_target_pairs={{0,1},{1,0},{2,3},{3,2},{4,7},{5,6},{6,5},{7,4},{8,9},{9,8},{10,11... | collective-permute-start | bytes 3145736 | tf_op jit(solution)/shard_map/ppermute | solution.py:51
  61.7 94.2 %collective-permute-start.14 = (bf16[1024,512]{1,0:T(8,128)(2,1)}, bf16[1024,512]{1,0:T(8,128)(2,1)}, u32[]{:S(2)}, u32[]{:S(2)}) collective-permute-start(bf16[1024,512]{1,0:T(8,128)(2,1)} %get-tuple-element.22), channel_id=1, source_target_pairs={{0,1},{1,0},{2,3},{3,2},{4,7},{5,6},{6,5},{7,4},{8,9},{9,8},{10,11... | collective-permute-start | bytes 3145736 | tf_op jit(solution)/shard_map/ppermute | solution.py:51
  100.5 34.1 %copy-start.9 = (bf16[4096,256]{1,0:T(8,128)(2,1)}, bf16[4096,256]{1,0:T(8,128)(2,1)S(1)}, u32[]{:S(2)}) copy-start(bf16[4096,256]{1,0:T(8,128)(2,1)S(1)} %collective-permute-done.10.gate_part) | copy-start | bytes 6291460
  126.3 8.3 %copy-start.10 = (bf16[4096,256]{1,0:T(8,128)(2,1)}, bf16[4096,256]{1,0:T(8,128)(2,1)S(1)}, u32[]{:S(2)}) copy-start(bf16[4096,256]{1,0:T(8,128)(2,1)S(1)} %collective-permute-done.11.up_part) | copy-start | bytes 6291460
  134.6 21.3 %collective-permute-start.12 = (bf16[512,512]{1,0:T(8,128)(2,1)}, bf16[512,512]{1,0:T(8,128)(2,1)}, u32[]{:S(2)}, u32[]{:S(2)}) collective-permute-start(bf16[512,512]{1,0:T(8,128)(2,1)} %hidden.2.near), channel_id=1, source_target_pairs={{0,3},{1,2},{2,1},{3,0},{4,5},{5,4},{6,7},{7,6},{8,11},{9,10},{10,... | collective-permute-start | bytes 1572872 | tf_op jit(solution)/shard_map/ppermute | solution.py:51
  136.0 43.2 %collective-permute-start = (bf16[32,2048]{1,0:T(8,128)(2,1)S(1)}, bf16[32,2048]{1,0:T(8,128)(2,1)S(1)}, u32[]{:S(2)}, u32[]{:S(2)}) collective-permute-start(bf16[32,2048]{1,0:T(8,128)(2,1)S(1)} %multiply_convert_fusion), channel_id=1, source_target_pairs={{0,1},{1,2},{2,3},{3,4},{4,5},{5,6},{6,7},{7,8},{8,9},{9,10},{10,1... | collective-permute-start | bytes 393224 | tf_op jit(solution)/shard_map/ppermute | solution.py:443
  161.2 1.3 copy-start.2
  162.5 49.3 %all-to-all-start.1 = ((bf16[16,32,2048]{2,1,0:T(8,128)(2,1)}), bf16[16,32,2048]{2,1,0:T(8,128)(2,1)}, u32[]{:S(2)}, u32[]{:S(2)}) async-start(bf16[16,32,2048]{2,1,0:T(8,128)(2,1)} %copy-done.2), calls=%async_computation.1 | async-start | bytes 4194304 | tf_op jit(solution)/shard_map/all_to_all | solution.py:55
  169.3 9.9 %copy-start.12 = (f32[31,2048]{1,0:T(8,128)S(1)}, f32[31,2048]{1,0:T(8,128)}, u32[]{:S(2)}) copy-start(f32[31,2048]{1,0:T(8,128)} %taps_ref.1) | copy-start | bytes 761860
  169.3 9.9 %copy-start.13 = (f32[2048]{0:T(1024)S(1)}, f32[2048]{0:T(1024)}, u32[]{:S(2)}) copy-start(f32[2048]{0:T(1024)} %param.17) | copy-start | bytes 24580
  169.3 9.9 %copy-start.14 = (f32[2048]{0:T(1024)S(1)}, f32[2048]{0:T(1024)}, u32[]{:S(2)}) copy-start(f32[2048]{0:T(1024)} %param.18) | copy-start | bytes 24580
  179.2 24.7 %collective-permute-start.16 = (bf16[512,512]{1,0:T(8,128)(2,1)}, bf16[512,512]{1,0:T(8,128)(2,1)S(1)}, u32[]{:S(2)}, u32[]{:S(2)}) collective-permute-start(bf16[512,512]{1,0:T(8,128)(2,1)} %hidden.3.near), channel_id=1, source_target_pairs={{0,3},{1,2},{2,1},{3,0},{4,5},{5,4},{6,7},{7,6},{8,11},{9,10},{10,... | collective-permute-start | bytes 1572872 | tf_op jit(solution)/shard_map/ppermute | solution.py:51
  179.2 1.4 copy-start.3
  180.6 1.4 copy-start.4
  182.0 19.6 %copy-start.23 = (bf16[2048,1024]{1,0:T(8,128)(2,1)S(1)}, bf16[2048,1024]{1,0:T(8,128)(2,1)}, u32[]{:S(2)}) copy-start(bf16[2048,1024]{1,0:T(8,128)(2,1)} %param.19) | copy-start | bytes 12582916
  196.6 37.0 %collective-permute-start.2 = (bf16[192,2048]{1,0:T(8,128)(2,1)}, bf16[192,2048]{1,0:T(8,128)(2,1)}, u32[]{:S(2)}, u32[]{:S(2)}) collective-permute-start(bf16[192,2048]{1,0:T(8,128)(2,1)} %get-tuple-element.15), channel_id=1, source_target_pairs={{0,3},{1,0},{2,1},{3,2},{4,7},{5,4},{6,5},{7,6},{8,11},{9,8},{10,9... | collective-permute-start | bytes 2359304 | tf_op jit(solution)/shard_map/ppermute | solution.py:470
  198.5 43.6 %collective-permute-start.3 = (bf16[192,2048]{1,0:T(8,128)(2,1)}, bf16[192,2048]{1,0:T(8,128)(2,1)}, u32[]{:S(2)}, u32[]{:S(2)}) collective-permute-start(bf16[192,2048]{1,0:T(8,128)(2,1)} %get-tuple-element.15), channel_id=1, source_target_pairs={{0,1},{1,2},{2,3},{3,0},{4,5},{5,6},{6,7},{7,4},{8,9},{9,10},{10,1... | collective-permute-start | bytes 2359304 | tf_op jit(solution)/shard_map/ppermute | solution.py:470
  198.5 35.1 %collective-permute-start.1 = (bf16[192,2048]{1,0:T(8,128)(2,1)}, bf16[192,2048]{1,0:T(8,128)(2,1)}, u32[]{:S(2)}, u32[]{:S(2)}) collective-permute-start(bf16[192,2048]{1,0:T(8,128)(2,1)} %get-tuple-element.14), channel_id=1, source_target_pairs={{0,1},{1,2},{2,3},{3,0},{4,5},{5,6},{6,7},{7,4},{8,9},{9,10},{10,1... | collective-permute-start | bytes 2359304 | tf_op jit(solution)/shard_map/ppermute | solution.py:470
  199.5 45.5 %collective-permute-start.4 = (bf16[192,2048]{1,0:T(8,128)(2,1)}, bf16[192,2048]{1,0:T(8,128)(2,1)}, u32[]{:S(2)}, u32[]{:S(2)}) collective-permute-start(bf16[192,2048]{1,0:T(8,128)(2,1)} %get-tuple-element.14), channel_id=1, source_target_pairs={{0,3},{1,0},{2,1},{3,2},{4,7},{5,4},{6,5},{7,6},{8,11},{9,8},{10,9... | collective-permute-start | bytes 2359304 | tf_op jit(solution)/shard_map/ppermute | solution.py:470
  201.6 3.9 %copy-start.6 = (s32[8]{0:T(128)S(1)}, s32[8]{0:T(128)}, u32[]{:S(2)}) copy-start(s32[8]{0:T(128)} %stack.43.where) | copy-start | bytes 100
  201.6 3.9 %copy-start.11 = (bf16[512,512]{1,0:T(8,128)(2,1)S(1)}, bf16[512,512]{1,0:T(8,128)(2,1)}, u32[]{:S(2)}) copy-start(bf16[512,512]{1,0:T(8,128)(2,1)} %hidden.3.near) | copy-start | bytes 1572868
  203.8 1.7 copy-start.19
  210.5 1.4 copy-start.1
  211.9 40.2 %all-to-all-start.3 = ((bf16[16,32,2048]{2,1,0:T(8,128)(2,1)}), bf16[16,32,2048]{2,1,0:T(8,128)(2,1)S(1)}, u32[]{:S(2)}, u32[]{:S(2)}) async-start(bf16[16,32,2048]{2,1,0:T(8,128)(2,1)} %copy-done.1), calls=%async_computation.3 | async-start | bytes 4194304 | tf_op jit(solution)/shard_map/all_to_all | solution.py:55
  218.5 17.8 %copy-start.24 = (bf16[2048,1024]{1,0:T(8,128)(2,1)S(1)}, bf16[2048,1024]{1,0:T(8,128)(2,1)}, u32[]{:S(2)}) copy-start(bf16[2048,1024]{1,0:T(8,128)(2,1)} %param.19) | copy-start | bytes 12582916
  233.6 24.4 %collective-permute-start.5 = (bf16[192,2048]{1,0:T(8,128)(2,1)}, bf16[192,2048]{1,0:T(8,128)(2,1)}, u32[]{:S(2)}, u32[]{:S(2)}) collective-permute-start(bf16[192,2048]{1,0:T(8,128)(2,1)} %collective-permute-done.1), channel_id=1, source_target_pairs={{0,1},{1,2},{2,3},{3,0},{4,5},{5,6},{6,7},{7,4},{8,9},{9,10},{10,1... | collective-permute-start | bytes 2359304 | tf_op jit(solution)/shard_map/ppermute | solution.py:470
  233.6 27.3 %collective-permute-start.6 = (bf16[192,2048]{1,0:T(8,128)(2,1)}, bf16[192,2048]{1,0:T(8,128)(2,1)}, u32[]{:S(2)}, u32[]{:S(2)}) collective-permute-start(bf16[192,2048]{1,0:T(8,128)(2,1)} %collective-permute-done.2), channel_id=1, source_target_pairs={{0,3},{1,0},{2,1},{3,2},{4,7},{5,4},{6,5},{7,6},{8,11},{9,8},{10,9... | collective-permute-start | bytes 2359304 | tf_op jit(solution)/shard_map/ppermute | solution.py:470
  247.9 4.1 %copy-start.16 = (f32[4,512]{1,0:T(4,128)S(1)}, f32[4,512]{1,0:T(4,128)}, u32[]{:S(2)}) copy-start(f32[4,512]{1,0:T(4,128)} %copy-done.15) | copy-start | bytes 24580
  251.0 1.0 copy-start.17
  252.0 11.9 %collective-permute-start.15 = (bf16[256,1024]{1,0:T(8,128)(2,1)S(1)}, bf16[256,1024]{1,0:T(8,128)(2,1)S(1)}, u32[]{:S(2)}, u32[]{:S(2)}) collective-permute-start(bf16[256,1024]{1,0:T(8,128)(2,1)S(1)} %get-tuple-element.18), channel_id=1, source_target_pairs={{0,1},{1,0},{2,3},{3,2},{4,7},{5,6},{6,5},{7,4},{8,9},{9,8},{10,11... | collective-permute-start | bytes 1572872 | tf_op jit(solution)/shard_map/ppermute | solution.py:51
  252.0 5.9 %copy-start.25 = (bf16[2048,1024]{1,0:T(8,128)(2,1)S(1)}, bf16[2048,1024]{1,0:T(8,128)(2,1)}, u32[]{:S(2)}) copy-start(bf16[2048,1024]{1,0:T(8,128)(2,1)} %param.19) | copy-start | bytes 12582916
  254.1 9.8 %collective-permute-start.17 = (bf16[256,1024]{1,0:T(8,128)(2,1)S(1)}, bf16[256,1024]{1,0:T(8,128)(2,1)S(1)}, u32[]{:S(2)}, u32[]{:S(2)}) collective-permute-start(bf16[256,1024]{1,0:T(8,128)(2,1)S(1)} %get-tuple-element.20), channel_id=1, source_target_pairs={{0,4},{1,5},{2,6},{3,7},{4,0},{5,1},{6,2},{7,3},{8,12},{9,13},{10,... | collective-permute-start | bytes 1572872 | tf_op jit(solution)/shard_map/ppermute | solution.py:51
  257.9 12.0 %collective-permute-start.18 = (bf16[256,1024]{1,0:T(8,128)(2,1)S(1)}, bf16[256,1024]{1,0:T(8,128)(2,1)S(1)}, u32[]{:S(2)}, u32[]{:S(2)}) collective-permute-start(bf16[256,1024]{1,0:T(8,128)(2,1)S(1)} %get-tuple-element.21), channel_id=1, source_target_pairs={{0,5},{1,4},{2,7},{3,6},{4,3},{5,2},{6,1},{7,0},{8,13},{9,12},{10,... | collective-permute-start | bytes 1572872 | tf_op jit(solution)/shard_map/ppermute | solution.py:51
  260.9 9.1 %copy-start.18 = (f32[256,1024]{1,0:T(8,128)S(1)}, f32[256,1024]{1,0:T(8,128)}, u32[]{:S(2)}) copy-start(f32[256,1024]{1,0:T(8,128)} %copy-done.17) | copy-start | bytes 3145732
